TPU v7x, 1024 devices: a whole 4x8x16 slice. The times are simulated.
1024 devices in a mesh: ep: 32 (over z, core), tp: 32 (over y, x).
Axes of the slice: x: 4, y: 8, z: 16, core: 2. Of those that a mesh axis runs over, the one named last changes fastest.
Arguments:
- resid: bfloat16 [1024, 2048], P('ep', 'tp'), may hold values from -6 to 6
- cache_key: bfloat16 [1024, 8, 224, 256], P(('ep', 'tp')), may hold values from -360 to 360
- cache_value: bfloat16 [1024, 8, 224, 256], P(('ep', 'tp')), may hold values from -6 to 6
- lengths: int32 [1024], P(('ep', 'tp')), may hold values from 28 to 224
- lambdas: float32 [8], replicated, may hold values from 0.3 to 0.8
- mix_gain: float32 [2048], replicated, may hold values from 0.1 to 1.9
- query_gain: float32 [128], replicated, may hold values from 0.1 to 1.9
- key_gain: float32 [128], replicated, may hold values from 0.1 to 1.9
- sub_gain: float32 [256], replicated, may hold values from 0.1 to 1.9
- ffn_gain: float32 [2048], replicated, may hold values from 0.1 to 1.9
- w_query: bfloat16 [2048, 2048], P(None, 'tp'), may hold values from -0.125 to 0.125
- w_key: bfloat16 [2048, 2048], P(None, 'tp'), may hold values from -0.125 to 0.125
- w_value: bfloat16 [2048, 2048], P(None, 'tp'), may hold values from -0.125 to 0.125
- w_out: bfloat16 [2048, 2048], P(None, 'tp'), may hold values from -0.125 to 0.125
- routes: int32 [1024, 2], P('ep'), may hold values from 0 to 31, all different within a row; in each aligned block of 32 rows (0 to 31, 32 to 63, ...) at most 4 rows name the same one
- route_weights: float32 [1024, 2], P('ep'), may hold values from 0.2 to 0.8
- w_gate: bfloat16 [32, 2048, 4096], P('ep', None, 'tp'), may hold values from -0.125 to 0.125
- w_up: bfloat16 [32, 2048, 4096], P('ep', None, 'tp'), may hold values from -0.125 to 0.125
- w_down: bfloat16 [32, 4096, 2048], P('ep', 'tp'), may hold values from -0.09375 to 0.09375
Outputs:
- result: bfloat16 [1024, 2048], P('ep', 'tp')
- new_key: bfloat16 [1024, 8, 256], P(('ep', 'tp'))
- new_value: bfloat16 [1024, 8, 256], P(('ep', 'tp'))
Inputs may be any that keep to these rules, and one draw needn't show every extreme that they name: `routes`: within the 32 rows of one index of ep no expert is named more than 4 times, and in some of them one expert is named exactly 4 times; the two experts of a row differ. `lengths`: every sequence has at least two live positions.
All inputs are finite; a program needn't handle non-finite values.
Results may differ from a plain program's by a relative error of at most 0.0099.
Values may be sent and summed in bfloat16 or wider, within the bound.
No kernel may reach another device: no remote copies, remote signals or barrier semaphores. Data moves between devices by JAX's collectives and lax.ppermute only.
A program may use at most 32 MiB of HBM per device.

v0:
```python
import math

import jax
import jax.numpy as jnp
from jax import lax
from jax.sharding import PartitionSpec as P

CAP = 4


epsilon = 1e-06
out_factor = 0.2 + 0.6 * math.exp(-0.3)
masked_score = -1e30


def from_everyone(x, axis):
    copies = jnp.broadcast_to(x, (lax.axis_size(axis), *x.shape))
    return lax.all_to_all(copies, axis, split_axis=0, concat_axis=0, tiled=True)


def laid_out(pieces, dim):
    dims = list(pieces.shape[1:])
    dims[dim] *= pieces.shape[0]
    return jnp.moveaxis(pieces, 0, dim).reshape(dims)


def collect(x, axis, dim):
    pieces = from_everyone(x, axis)
    return laid_out(pieces, dim)


def cut_along(x, dim, size):
    before, after = (x.shape[:dim], x.shape[dim + 1 :])
    return jnp.moveaxis(x.reshape(*before, size, -1, *after), dim, 0)


def summed_on_arrival(x, axis, dim):
    pieces = cut_along(x, dim, lax.axis_size(axis))
    arrived = lax.all_to_all(pieces, axis, split_axis=0, concat_axis=0, tiled=True)
    return arrived.astype(jnp.float32).sum(axis=0)


def scaled_rows(values, gain):
    wide = values.astype(jnp.float32)
    return wide * lax.rsqrt(jnp.mean(wide * wide, axis=-1, keepdims=True) + epsilon) * gain


def route_tables(routes, route_weights, experts, capacity):
    flat_routes = routes.reshape(-1)
    expert_hit = (flat_routes[:, None] == jnp.arange(experts, dtype=jnp.int32)[None, :]).astype(
        jnp.int32
    )
    before = jnp.cumsum(expert_hit, axis=0) - expert_hit
    slot_index = jnp.sum(before * expert_hit, axis=1)
    slot_hit = (slot_index[:, None] == jnp.arange(capacity, dtype=jnp.int32)[None, :]).astype(
        jnp.float32
    )
    pair_table = expert_hit.astype(jnp.float32)[:, :, None] * slot_hit[:, None, :]
    pair_table = pair_table.reshape(routes.shape[0], 2, experts, capacity)
    dispatch = jnp.sum(pair_table, axis=1)
    combine = jnp.sum(pair_table * route_weights[:, :, None, None], axis=1)
    return (dispatch, combine)


def attend(
    queries,
    key_rows,
    value_rows,
    past_keys,
    past_values,
    live_len,
    lambdas,
    query_gain,
    key_gain,
    sub_gain,
):
    seq_count, kv_heads, cache_len, key_width = past_keys.shape
    head_dim = key_width // 2
    head_count = lambdas.shape[0]
    group_size = head_count // kv_heads
    value_dim = past_values.shape[-1]
    score_scale = head_dim ** (-0.5)
    q_unit = scaled_rows(
        queries.reshape(seq_count, kv_heads, group_size, 2, head_dim), query_gain
    ).astype(jnp.bfloat16)
    new_key = scaled_rows(key_rows.reshape(seq_count, kv_heads, 2, head_dim), key_gain).astype(
        jnp.bfloat16
    )
    new_value = value_rows.reshape(seq_count, kv_heads, value_dim)
    past_split = past_keys.reshape(seq_count, kv_heads, cache_len, 2, head_dim)
    scores = (
        jnp.einsum("sjgmd,sjlmd->sjgml", q_unit, past_split, preferred_element_type=jnp.float32)
        * score_scale
    )
    own_score = (
        jnp.einsum("sjgmd,sjmd->sjgm", q_unit, new_key, preferred_element_type=jnp.float32)
        * score_scale
    )
    live_mask = jnp.arange(cache_len, dtype=jnp.int32)[None, :] < live_len[:, None]
    scores = jnp.where(live_mask[:, None, None, None, :], scores, masked_score)
    peak = jnp.maximum(jnp.max(scores, axis=-1), own_score)
    past_weight = jnp.exp(scores - peak[..., None])
    own_weight = jnp.exp(own_score - peak)
    totals = jnp.sum(past_weight, axis=-1) + own_weight
    past_prob = past_weight / totals[..., None]
    own_prob = own_weight / totals
    mix_lambda = lambdas.reshape(1, kv_heads, group_size, 1)
    past_mix = (past_prob[..., 0, :] - mix_lambda * past_prob[..., 1, :]).astype(jnp.bfloat16)
    own_mix = (own_prob[..., 0] - mix_lambda[..., 0] * own_prob[..., 1]).astype(jnp.bfloat16)
    head_out = jnp.einsum(
        "sjgl,sjlv->sjgv", past_mix, past_values, preferred_element_type=jnp.float32
    )
    head_out = (
        head_out
        + own_mix.astype(jnp.float32)[..., None] * new_value.astype(jnp.float32)[:, :, None, :]
    )
    mixed = (
        (scaled_rows(head_out, sub_gain) * out_factor)
        .astype(jnp.bfloat16)
        .reshape(seq_count, head_count * value_dim)
    )
    return (mixed, new_key.reshape(seq_count, kv_heads, key_width), new_value)


def local(
    resid,
    cache_key,
    cache_value,
    lengths,
    lambdas,
    mix_gain,
    query_gain,
    key_gain,
    sub_gain,
    ffn_gain,
    w_query,
    w_key,
    w_value,
    w_out,
    routes,
    route_weights,
    w_gate,
    w_up,
    w_down,
):
    gathered = collect(resid, "tp", 1)
    normed = scaled_rows(gathered, mix_gain).astype(jnp.bfloat16)
    query_part = jnp.dot(normed, w_query, preferred_element_type=jnp.float32).astype(jnp.bfloat16)
    key_part = jnp.dot(normed, w_key, preferred_element_type=jnp.float32).astype(jnp.bfloat16)
    value_part = jnp.dot(normed, w_value, preferred_element_type=jnp.float32).astype(jnp.bfloat16)
    queries, key_rows, value_rows = (
        lax.all_to_all(query_part, "tp", split_axis=0, concat_axis=1, tiled=True),
        lax.all_to_all(key_part, "tp", split_axis=0, concat_axis=1, tiled=True),
        lax.all_to_all(value_part, "tp", split_axis=0, concat_axis=1, tiled=True),
    )
    mixed, new_key, new_value = attend(
        queries,
        key_rows,
        value_rows,
        cache_key,
        cache_value,
        lengths,
        lambdas,
        query_gain,
        key_gain,
        sub_gain,
    )
    attn_proj = jnp.dot(collect(mixed, "tp", 0), w_out, preferred_element_type=jnp.float32)
    updated = (resid.astype(jnp.float32) + attn_proj).astype(jnp.bfloat16)
    updated_rows = collect(updated, "tp", 1)
    hidden = scaled_rows(updated_rows, ffn_gain).astype(jnp.bfloat16)
    experts = w_gate.shape[0] * lax.axis_size("ep")
    dispatch, combine = route_tables(routes, route_weights, experts, CAP)
    send = jnp.einsum(
        "gec,gd->ecd", dispatch.astype(jnp.bfloat16), hidden, preferred_element_type=jnp.float32
    ).astype(jnp.bfloat16)
    slots = lax.all_to_all(send, "ep", split_axis=0, concat_axis=0, tiled=True)
    flat_rows = slots.reshape(-1, slots.shape[-1])
    gate_out = jnp.dot(flat_rows, w_gate[0], preferred_element_type=jnp.float32)
    up_out = jnp.dot(flat_rows, w_up[0], preferred_element_type=jnp.float32)
    act = (jax.nn.silu(gate_out) * up_out).astype(jnp.bfloat16)
    down_out = jnp.dot(act, w_down[0], preferred_element_type=jnp.float32)
    partial_value = down_out.reshape(slots.shape[0], slots.shape[1], down_out.shape[-1])
    flat_combine = combine.reshape(combine.shape[0], -1)
    summed = summed_on_arrival(partial_value.astype(jnp.bfloat16), "tp", 2)
    returned = lax.all_to_all(
        summed.astype(jnp.bfloat16), "ep", split_axis=0, concat_axis=0, tiled=True
    ).astype(summed.dtype)
    expert_mix = jnp.dot(
        flat_combine, returned.reshape(-1, returned.shape[-1]), preferred_element_type=jnp.float32
    )
    result = (updated.astype(jnp.float32) + expert_mix).astype(jnp.bfloat16)
    return (result, new_key, new_value)


def solution(mesh):
    in_specs = (
        P("ep", "tp"),
        P(("ep", "tp"), None, None, None),
        P(("ep", "tp"), None, None, None),
        P(("ep", "tp")),
        P(),
        P(),
        P(),
        P(),
        P(),
        P(),
        P(None, "tp"),
        P(None, "tp"),
        P(None, "tp"),
        P(None, "tp"),
        P("ep", None),
        P("ep", None),
        P("ep", None, "tp"),
        P("ep", None, "tp"),
        P("ep", "tp", None),
    )
    out_specs = (P("ep", "tp"), P(("ep", "tp"), None, None), P(("ep", "tp"), None, None))
    return jax.shard_map(local, mesh=mesh, in_specs=in_specs, out_specs=out_specs, check_vma=False)
```

profile of v0, /device:TPU:1, one launch (start us, length us, event | category | flops | bytes accessed | tf_op | source)
XLA Modules:
  0.0 206.4 jit_solution(649138533802291171)
XLA Ops:
  0.7 0.9 broadcast_in_dim.19
  1.5 0.8 reshape.423
  2.4 10.5 %all-to-all-start = ((bf16[32,2,1024]{2,1,0:T(2,128)(2,1)}), bf16[32,2,1024]{2,1,0:T(2,128)(2,1)S(1)}, u32[]{:S(2)}, u32[]{:S(2)}) async-start(bf16[32,2,1024]{2,1,0:T(2,128)(2,1)} %reshape.423), calls=%async_computation | async-start | bytes 262144 | tf_op jit(solution)/shard_map/all_to_all | solution.py:18
  14.1 8.1 %all-to-all-done = bf16[32,2,1024]{2,1,0:T(2,128)(2,1)S(1)} async-done(((bf16[32,2,1024]{2,1,0:T(2,128)(2,1)}), bf16[32,2,1024]{2,1,0:T(2,128)(2,1)S(1)}, u32[]{:S(2)}, u32[]{:S(2)}) %all-to-all-start) | async-done | bytes 131104 | tf_op jit(solution)/shard_map/all_to_all | solution.py:18
  23.8 0.9 copy-done.4
  25.5 3.8 %all-to-all-start.1 = ((bf16[32,1,64]{2,1,0:T(2,128)(2,1)}), bf16[32,1,64]{2,1,0:T(2,128)(2,1)S(1)}, u32[]{:S(2)}, u32[]{:S(2)}) async-start(bf16[32,1,64]{2,1,0:T(2,128)(2,1)} %copy.83), calls=%async_computation.1 | async-start | bytes 32768 | tf_op jit(solution)/shard_map/all_to_all | solution.py:152
  30.1 7.6 %all-to-all-done.1 = bf16[32,1,64]{2,1,0:T(2,128)(2,1)S(1)} async-done(((bf16[32,1,64]{2,1,0:T(2,128)(2,1)}), bf16[32,1,64]{2,1,0:T(2,128)(2,1)S(1)}, u32[]{:S(2)}, u32[]{:S(2)}) %all-to-all-start.1) | async-done | bytes 4128 | tf_op jit(solution)/shard_map/all_to_all | solution.py:152
  37.7 3.9 %all-to-all-start.3 = ((bf16[32,1,64]{2,1,0:T(2,128)(2,1)}), bf16[32,1,64]{2,1,0:T(2,128)(2,1)S(1)}, u32[]{:S(2)}, u32[]{:S(2)}) async-start(bf16[32,1,64]{2,1,0:T(2,128)(2,1)} %copy.85), calls=%async_computation.3 | async-start | bytes 32768 | tf_op jit(solution)/shard_map/all_to_all | solution.py:154
  42.4 7.8 %all-to-all-done.3 = bf16[32,1,64]{2,1,0:T(2,128)(2,1)S(1)} async-done(((bf16[32,1,64]{2,1,0:T(2,128)(2,1)}), bf16[32,1,64]{2,1,0:T(2,128)(2,1)S(1)}, u32[]{:S(2)}, u32[]{:S(2)}) %all-to-all-start.3) | async-done | bytes 4128 | tf_op jit(solution)/shard_map/all_to_all | solution.py:154
  50.2 3.8 %all-to-all-start.2 = ((bf16[32,1,64]{2,1,0:T(2,128)(2,1)}), bf16[32,1,64]{2,1,0:T(2,128)(2,1)S(1)}, u32[]{:S(2)}, u32[]{:S(2)}) async-start(bf16[32,1,64]{2,1,0:T(2,128)(2,1)} %copy.84), calls=%async_computation.2 | async-start | bytes 32768 | tf_op jit(solution)/shard_map/all_to_all | solution.py:153
  54.4 8.0 %all-to-all-done.2 = bf16[32,1,64]{2,1,0:T(2,128)(2,1)S(1)} async-done(((bf16[32,1,64]{2,1,0:T(2,128)(2,1)}), bf16[32,1,64]{2,1,0:T(2,128)(2,1)S(1)}, u32[]{:S(2)}, u32[]{:S(2)}) %all-to-all-start.2) | async-done | bytes 4128 | tf_op jit(solution)/shard_map/all_to_all | solution.py:153
  67.1 1.4 reduce.40
  69.2 3.9 %all-to-all-start.4 = ((bf16[32,2,1024]{2,1,0:T(2,128)(2,1)}), bf16[32,2,1024]{2,1,0:T(2,128)(2,1)S(1)}, u32[]{:S(2)}, u32[]{:S(2)}) async-start(bf16[32,2,1024]{2,1,0:T(2,128)(2,1)} %reshape.425), calls=%async_computation.4 | async-start | bytes 262144 | tf_op jit(solution)/shard_map/all_to_all | solution.py:18
  73.5 8.9 %all-to-all-done.4 = bf16[32,2,1024]{2,1,0:T(2,128)(2,1)S(1)} async-done(((bf16[32,2,1024]{2,1,0:T(2,128)(2,1)}), bf16[32,2,1024]{2,1,0:T(2,128)(2,1)S(1)}, u32[]{:S(2)}, u32[]{:S(2)}) %all-to-all-start.4) | async-done | bytes 131104 | tf_op jit(solution)/shard_map/all_to_all | solution.py:18
  83.6 3.9 %all-to-all-start.5 = ((bf16[32,2,1024]{2,1,0:T(2,128)(2,1)}), bf16[32,2,1024]{2,1,0:T(2,128)(2,1)S(1)}, u32[]{:S(2)}, u32[]{:S(2)}) async-start(bf16[32,2,1024]{2,1,0:T(2,128)(2,1)} %reshape.427), calls=%async_computation.5 | async-start | bytes 262144 | tf_op jit(solution)/shard_map/all_to_all | solution.py:18
  88.3 8.6 %all-to-all-done.5 = bf16[32,2,1024]{2,1,0:T(2,128)(2,1)S(1)} async-done(((bf16[32,2,1024]{2,1,0:T(2,128)(2,1)}), bf16[32,2,1024]{2,1,0:T(2,128)(2,1)S(1)}, u32[]{:S(2)}, u32[]{:S(2)}) %all-to-all-start.5) | async-done | bytes 131104 | tf_op jit(solution)/shard_map/all_to_all | solution.py:18
  99.2 60.2 %all_to_all.69 = bf16[32,4,2048]{2,1,0:T(4,128)(2,1)S(1)} all-to-all(bf16[32,4,2048]{2,1,0:T(4,128)(2,1)S(1)} %copy.90), channel_id=1, replica_groups=mesh['ep'=32,'tp'=32] {'ep'}, dimensions={0} | all-to-all | bytes 1048576 | tf_op jit(solution)/shard_map/all_to_all | solution.py:177
  159.5 0.9 copy-done.2
  162.8 1.1 reshape.375
  164.3 1.5 reshape.429
  165.8 3.9 %all-to-all-start.7 = ((bf16[32,2,4096]{2,1,0:T(2,128)(2,1)}), bf16[32,2,4096]{2,1,0:T(2,128)(2,1)S(1)}, u32[]{:S(2)}, u32[]{:S(2)}) async-start(bf16[32,2,4096]{2,1,0:T(2,128)(2,1)} %reshape.429), calls=%async_computation.7 | async-start | bytes 1048576 | tf_op jit(solution)/shard_map/all_to_all | solution.py:39
  169.9 16.4 %all-to-all-done.7 = bf16[32,2,4096]{2,1,0:T(2,128)(2,1)S(1)} async-done(((bf16[32,2,4096]{2,1,0:T(2,128)(2,1)}), bf16[32,2,4096]{2,1,0:T(2,128)(2,1)S(1)}, u32[]{:S(2)}, u32[]{:S(2)}) %all-to-all-start.7) | async-done | bytes 524320 | tf_op jit(solution)/shard_map/all_to_all | solution.py:39
  187.9 5.7 %all-to-all-start.8 = ((bf16[32,2,128]{2,1,0:T(2,128)(2,1)}), bf16[32,2,128]{2,1,0:T(2,128)(2,1)S(1)}, u32[]{:S(2)}, u32[]{:S(2)}) async-start(bf16[32,2,128]{2,1,0:T(2,128)(2,1)} %reshape.431), calls=%async_computation.8 | async-start | bytes 32768 | tf_op jit(solution)/shard_map/all_to_all | solution.py:186
  194.9 10.6 %all-to-all-done.8 = bf16[32,2,128]{2,1,0:T(2,128)(2,1)S(1)} async-done(((bf16[32,2,128]{2,1,0:T(2,128)(2,1)}), bf16[32,2,128]{2,1,0:T(2,128)(2,1)S(1)}, u32[]{:S(2)}, u32[]{:S(2)}) %all-to-all-start.8) | async-done | bytes 16416 | tf_op jit(solution)/shard_map/all_to_all | solution.py:186
  (119 shorter events, 21.8 us)
Async XLA Ops:
  0.6 64.6 %copy-start = (bf16[1,8,224,256]{3,2,1,0:T(8,128)(2,1)S(1)}, bf16[1,8,224,256]{3,2,1,0:T(8,128)(2,1)}, u32[]{:S(2)}) copy-start(bf16[1,8,224,256]{3,2,1,0:T(8,128)(2,1)} %param.21) | copy-start | bytes 2752516
  0.6 13.1 %copy-start.1 = (bf16[1,8,224,256]{3,2,1,0:T(8,128)(2,1)S(1)}, bf16[1,8,224,256]{3,2,1,0:T(8,128)(2,1)}, u32[]{:S(2)}) copy-start(bf16[1,8,224,256]{3,2,1,0:T(8,128)(2,1)} %param.20) | copy-start | bytes 2752516
  2.4 19.8 %all-to-all-start = ((bf16[32,2,1024]{2,1,0:T(2,128)(2,1)}), bf16[32,2,1024]{2,1,0:T(2,128)(2,1)S(1)}, u32[]{:S(2)}, u32[]{:S(2)}) async-start(bf16[32,2,1024]{2,1,0:T(2,128)(2,1)} %reshape.423), calls=%async_computation | async-start | bytes 262144 | tf_op jit(solution)/shard_map/all_to_all | solution.py:18
  12.8 0.7 copy-start.11
  23.0 0.7 copy-start.10
  23.7 0.9 copy-start.4
  24.7 4.6 %copy-start.5 = (bf16[2048,64]{0,1:T(8,128)(2,1)S(1)}, bf16[2048,64]{0,1:T(8,128)(2,1)}, u32[]{:S(2)}) copy-start(bf16[2048,64]{0,1:T(8,128)(2,1)} %param.31) | copy-start | bytes 786436
  24.8 16.7 %copy-start.6 = (bf16[2048,64]{0,1:T(8,128)(2,1)S(1)}, bf16[2048,64]{0,1:T(8,128)(2,1)}, u32[]{:S(2)}) copy-start(bf16[2048,64]{0,1:T(8,128)(2,1)} %param.30) | copy-start | bytes 786436
  25.5 12.2 %all-to-all-start.1 = ((bf16[32,1,64]{2,1,0:T(2,128)(2,1)}), bf16[32,1,64]{2,1,0:T(2,128)(2,1)S(1)}, u32[]{:S(2)}, u32[]{:S(2)}) async-start(bf16[32,1,64]{2,1,0:T(2,128)(2,1)} %copy.83), calls=%async_computation.1 | async-start | bytes 32768 | tf_op jit(solution)/shard_map/all_to_all | solution.py:152
  37.7 12.5 %all-to-all-start.3 = ((bf16[32,1,64]{2,1,0:T(2,128)(2,1)}), bf16[32,1,64]{2,1,0:T(2,128)(2,1)S(1)}, u32[]{:S(2)}, u32[]{:S(2)}) async-start(bf16[32,1,64]{2,1,0:T(2,128)(2,1)} %copy.85), calls=%async_computation.3 | async-start | bytes 32768 | tf_op jit(solution)/shard_map/all_to_all | solution.py:154
  50.2 12.2 %all-to-all-start.2 = ((bf16[32,1,64]{2,1,0:T(2,128)(2,1)}), bf16[32,1,64]{2,1,0:T(2,128)(2,1)S(1)}, u32[]{:S(2)}, u32[]{:S(2)}) async-start(bf16[32,1,64]{2,1,0:T(2,128)(2,1)} %copy.84), calls=%async_computation.2 | async-start | bytes 32768 | tf_op jit(solution)/shard_map/all_to_all | solution.py:153
  64.5 0.7 copy-start.12
  65.6 0.7 copy-start.14
  69.2 13.3 %all-to-all-start.4 = ((bf16[32,2,1024]{2,1,0:T(2,128)(2,1)}), bf16[32,2,1024]{2,1,0:T(2,128)(2,1)S(1)}, u32[]{:S(2)}, u32[]{:S(2)}) async-start(bf16[32,2,1024]{2,1,0:T(2,128)(2,1)} %reshape.425), calls=%async_computation.4 | async-start | bytes 262144 | tf_op jit(solution)/shard_map/all_to_all | solution.py:18
  73.0 9.5 %copy-start.7 = (bf16[2048,64]{0,1:T(8,128)(2,1)S(1)}, bf16[2048,64]{0,1:T(8,128)(2,1)}, u32[]{:S(2)}) copy-start(bf16[2048,64]{0,1:T(8,128)(2,1)} %param.32) | copy-start | bytes 786436
  73.5 9.1 %copy-start.8 = (bf16[32,64]{1,0:T(8,128)(2,1)S(1)}, bf16[32,64]{1,0:T(8,128)(2,1)}, u32[]{:S(2)}) copy-start(bf16[32,64]{1,0:T(8,128)(2,1)} %param.19) | copy-start | bytes 12292
  83.6 13.3 %all-to-all-start.5 = ((bf16[32,2,1024]{2,1,0:T(2,128)(2,1)}), bf16[32,2,1024]{2,1,0:T(2,128)(2,1)S(1)}, u32[]{:S(2)}, u32[]{:S(2)}) async-start(bf16[32,2,1024]{2,1,0:T(2,128)(2,1)} %reshape.427), calls=%async_computation.5 | async-start | bytes 262144 | tf_op jit(solution)/shard_map/all_to_all | solution.py:18
  87.5 0.7 copy-start.13
  97.7 0.7 copy-start.9
  159.4 1.0 copy-start.2
  160.4 1.0 copy-start.17
  161.5 1.0 copy-start.3
  165.8 20.5 %all-to-all-start.7 = ((bf16[32,2,4096]{2,1,0:T(2,128)(2,1)}), bf16[32,2,4096]{2,1,0:T(2,128)(2,1)S(1)}, u32[]{:S(2)}, u32[]{:S(2)}) async-start(bf16[32,2,4096]{2,1,0:T(2,128)(2,1)} %reshape.429), calls=%async_computation.7 | async-start | bytes 1048576 | tf_op jit(solution)/shard_map/all_to_all | solution.py:39
  187.9 17.6 %all-to-all-start.8 = ((bf16[32,2,128]{2,1,0:T(2,128)(2,1)}), bf16[32,2,128]{2,1,0:T(2,128)(2,1)S(1)}, u32[]{:S(2)}, u32[]{:S(2)}) async-start(bf16[32,2,128]{2,1,0:T(2,128)(2,1)} %reshape.431), calls=%async_computation.8 | async-start | bytes 32768 | tf_op jit(solution)/shard_map/all_to_all | solution.py:186
  (2 other events, 1.3 us)
where the time goes:
time: 207 us; the launch traced here: 206 us
  waiting for transfers between devices  76 us (37%)
  blocking collectives  60.2 us (29%)
  starting transfers between devices  39.1 us (19%)
  local copies, waits for them, and re-layouts  21.1 us (10%)
  other arithmetic  4.67 us (2%)
  matrix products  3.55 us (2%)
    all_to_all x1, blocking collectives, local(): slots = lax.all_to_all(send, 'ep', split_axis=0, concat_axis=0, tiled=True)  60.2 us
    all_to_all x3, waiting for transfers between devices, from_everyone(): return lax.all_to_all(copies, axis, split_axis=0, concat_axis=0, tiled=True)  25.6 us
    all_to_all x3, starting transfers between devices, from_everyone(): return lax.all_to_all(copies, axis, split_axis=0, concat_axis=0, tiled=True)  18.2 us
    all_to_all x1, waiting for transfers between devices, summed_on_arrival(): lax.all_to_all(pieces, axis, split_axis=0, concat_axis=0, tiled=True)  16.4 us
    unnamed x48, local copies, waits for them, and re-layouts  12.8 us
    all_to_all x1, waiting for transfers between devices, local(): lax.all_to_all(summed.astype(jnp.bfloat16), 'ep', split_axis=0, concat_ax...  10.6 us
    all_to_all x1, waiting for transfers between devices, local(): lax.all_to_all(key_part, 'tp', split_axis=0, concat_axis=1, tiled=True)  7.98 us
    all_to_all x1, waiting for transfers between devices, local(): lax.all_to_all(value_part, 'tp', split_axis=0, concat_axis=1, tiled=True)  7.79 us
  transfers between devices with their start and end apart: 8, of which 8 were waited for; matrix products, arithmetic and copies ran while one was open for 2% of the time, Pallas kernels for 0%

commit v1 on v0

v1 whole, which is shorter than its diff:
```python
import math

import jax
import jax.numpy as jnp
from jax import lax
from jax.experimental import pallas as pl
from jax.experimental.pallas import tpu as pltpu
from jax.sharding import PartitionSpec as P

CAP = 4
EPS = 1e-06
OUT_FACTOR = 0.2 + 0.6 * math.exp(-0.3)
MASKED = -1e30

f32 = jnp.float32
bf16 = jnp.bfloat16

VMEM = pl.BlockSpec(memory_space=pltpu.VMEM)
SMEM = pl.BlockSpec(memory_space=pltpu.SMEM)


def nt(a, b):
    return lax.dot_general(a, b, (((1,), (1,)), ((), ())), preferred_element_type=f32)


def nn(a, b):
    return lax.dot_general(a, b, (((1,), (0,)), ((), ())), preferred_element_type=f32)


def tn(a, b):
    return lax.dot_general(a, b, (((0,), (0,)), ((), ())), preferred_element_type=f32)


def left_half(shape):
    return lax.broadcasted_iota(jnp.int32, shape, len(shape) - 1) < 64


def swap(x):
    return pltpu.roll(x, 64, 1)


def pack_kernel(x_ref, o_ref):
    x = x_ref[...].astype(f32)
    o_ref[...] = jnp.concatenate([x[:16], x[16:]], axis=1).astype(bf16)


def qkv_kernel(x_ref, gain_ref, wq_ref, wk_ref, wv_ref, o_ref, s_ref):
    tp = x_ref.shape[0] // 16
    left = left_half((16, 128))
    tiles = []
    total = jnp.zeros((32, 128), f32)
    for i in range(tp // 2):
        a = x_ref[32 * i : 32 * i + 16, :].astype(f32)
        b = x_ref[32 * i + 16 : 32 * i + 32, :].astype(f32)
        tile = jnp.concatenate(
            [jnp.where(left, a, swap(b)), jnp.where(left, swap(a), b)], axis=0
        )
        total = total + tile * tile
        tiles.append(tile)
    width = 64.0 * tp
    scale = lax.rsqrt(jnp.sum(total, axis=1, keepdims=True) / width + EPS)
    normed = jnp.concatenate(
        [(tile * scale * gain_ref[i : i + 1, :]).astype(bf16) for i, tile in enumerate(tiles)],
        axis=1,
    )
    q = nt(normed, wq_ref[...])
    k = nt(normed, wk_ref[...])
    v = nt(normed, wv_ref[...])
    s_ref[pl.ds(0, 32, stride=2), :] = jnp.concatenate([q, k], axis=1)
    s_ref[pl.ds(1, 32, stride=2), :] = jnp.concatenate([v, jnp.zeros_like(v)], axis=1)
    o_ref[...] = s_ref[...].astype(bf16)


def attend_kernel(
    len_ref, lam_ref, x_ref, ck_ref, cv_ref, qg_ref, kg_ref, sg_ref, o_ref, nk_ref, nv_ref, s_ref, p_ref
):
    heads, length, width = ck_ref.shape
    s_ref[...] = x_ref[...].astype(f32)
    rows = 2 * heads
    qk_even = s_ref[pl.ds(0, rows, stride=4), :]
    v_even = s_ref[pl.ds(1, rows, stride=4), :]
    qk_odd = s_ref[pl.ds(2, rows, stride=4), :]
    v_odd = s_ref[pl.ds(3, rows, stride=4), :]
    left = left_half((rows, 128))
    q = jnp.where(left, qk_even, swap(qk_odd))
    k = jnp.where(left, swap(qk_even), qk_odd)
    v = jnp.where(left, v_even, swap(v_odd))

    def unit(z, gain):
        r = lax.rsqrt(jnp.mean(z * z, axis=1, keepdims=True) + EPS)
        return (z * r * gain).astype(bf16).astype(f32)

    qu = unit(q, qg_ref[...])
    ku = unit(k, kg_ref[...])
    s_ref[0:rows, :] = ku
    s_ref[rows : 2 * rows, :] = v
    new_key = jnp.concatenate(
        [s_ref[pl.ds(0, heads, stride=2), :], s_ref[pl.ds(1, heads, stride=2), :]], axis=1
    )
    new_value = jnp.concatenate(
        [s_ref[pl.ds(rows, heads, stride=2), :], s_ref[pl.ds(rows + 1, heads, stride=2), :]], axis=1
    )
    nk_ref[...] = new_key.astype(bf16)
    nv_ref[...] = new_value.astype(bf16)

    row = lax.broadcasted_iota(jnp.int32, (rows, 1), 0)
    first_map = (row % 2) == 0
    wide = jnp.concatenate(
        [jnp.where(first_map, qu, 0.0), jnp.where(first_map, 0.0, qu)], axis=1
    )
    scores = jnp.zeros((rows, length), f32)
    for h in range(heads):
        lhs = jnp.where(row // 2 == h, wide, 0.0).astype(bf16)
        scores = scores + nt(lhs, ck_ref[h])
    scale = 128.0 ** -0.5
    scores = scores * scale
    own = jnp.sum(qu * ku, axis=1, keepdims=True) * scale
    live = lax.broadcasted_iota(jnp.int32, (rows, length), 1) < len_ref[0]
    scores = jnp.where(live, scores, MASKED)
    peak = jnp.maximum(jnp.max(scores, axis=1, keepdims=True), own)
    weight = jnp.exp(scores - peak)
    own_weight = jnp.exp(own - peak)
    totals = jnp.sum(weight, axis=1, keepdims=True) + own_weight
    prob = weight / totals
    p_ref[0] = prob[:, 0:128]
    p_ref[1] = jnp.concatenate([prob[:, 128:length], jnp.zeros((rows, 256 - length), f32)], axis=1)
    p_ref[2] = jnp.broadcast_to(own_weight / totals, (rows, 128))
    head = lax.broadcasted_iota(jnp.int32, (heads, 1), 0)
    lam = jnp.zeros((heads, 1), f32)
    for h in range(heads):
        lam = jnp.where(head == h, lam_ref[h], lam)
    mixes = [
        p_ref[pl.ds(j, 1), pl.ds(0, heads, stride=2), :][0] - lam * p_ref[pl.ds(j, 1), pl.ds(1, heads, stride=2), :][0]
        for j in range(3)
    ]
    past_mix = jnp.concatenate(mixes[:2], axis=1)[:, 0:length]
    own_mix = mixes[2][:, 0:1].astype(bf16).astype(f32)
    out = own_mix * new_value.astype(bf16).astype(f32)
    for h in range(heads):
        lhs = jnp.where(head == h, past_mix, 0.0).astype(bf16)
        out = out + nn(lhs, cv_ref[h])
    r = lax.rsqrt(jnp.mean(out * out, axis=1, keepdims=True) + EPS)
    o_ref[...] = (out * r * sg_ref[...] * OUT_FACTOR).astype(bf16)


def slot_table(routes_ref, experts, rows):
    hit_row = jnp.concatenate([routes_ref[0:1, :], routes_ref[1:2, :]], axis=1)
    pairs = hit_row.shape[1]
    hit = (lax.broadcasted_iota(jnp.int32, (experts, pairs), 0) == hit_row).astype(f32)
    upper = (
        lax.broadcasted_iota(jnp.int32, (pairs, pairs), 0)
        < lax.broadcasted_iota(jnp.int32, (pairs, pairs), 1)
    ).astype(bf16)
    before = nn(hit.astype(bf16), upper)
    slot = jnp.sum(before * hit, axis=0, keepdims=True).astype(jnp.int32)
    place = hit_row * 2 + slot // 2
    at = lax.broadcasted_iota(jnp.int32, (rows, pairs), 0) == place
    return [(at & (slot % 2 == half)).astype(f32) for half in (0, 1)]


def project_kernel(x_ref, w_ref, r_ref, routes_ref, u_ref, o_ref, s_ref):
    seqs = r_ref.shape[0]
    heads = x_ref.shape[0] // seqs
    width = x_ref.shape[1]
    for j in range(2):
        s_ref[j] = x_ref[:, 128 * j : 128 * (j + 1)].astype(f32)
    acc = r_ref[...].astype(f32)
    mixed = jnp.concatenate(
        [
            s_ref[pl.ds(j, 1), pl.ds(h, seqs, stride=heads), :][0].astype(bf16)
            for h in range(heads)
            for j in range(2)
        ],
        axis=1,
    )
    acc = acc + nt(mixed, w_ref[...])
    updated = acc.astype(bf16)
    u_ref[...] = updated
    rows = o_ref.shape[0]
    tables = slot_table(routes_ref, rows // 2, rows)
    halves = [nn((t[:, :seqs] + t[:, seqs:]).astype(bf16), updated) for t in tables]
    o_ref[...] = jnp.concatenate(halves, axis=1).astype(bf16)


def expert_kernel(x_ref, gain_ref, wg_ref, wu_ref, wd_ref, o_ref):
    rows = 64
    tp = x_ref.shape[0] // rows
    left = left_half((rows, 128))
    tiles = []
    total = jnp.zeros((2 * rows, 128), f32)
    for i in range(tp // 2):
        a = x_ref[2 * rows * i : 2 * rows * i + rows, :].astype(f32)
        b = x_ref[2 * rows * i + rows : 2 * rows * (i + 1), :].astype(f32)
        tile = jnp.concatenate(
            [jnp.where(left, a, swap(b)), jnp.where(left, swap(a), b)], axis=0
        )
        total = total + tile * tile
        tiles.append(tile)
    scale = lax.rsqrt(jnp.sum(total, axis=1, keepdims=True) / (64.0 * tp) + EPS)
    hidden = jnp.concatenate(
        [(tile * scale * gain_ref[i : i + 1, :]).astype(bf16) for i, tile in enumerate(tiles)],
        axis=1,
    )
    gate = nn(hidden, wg_ref[...])
    up = nn(hidden, wu_ref[...])
    act = (gate / (1.0 + jnp.exp(-gate)) * up).astype(bf16)
    for i in range(tp // 2):
        out = nn(act, wd_ref[:, 128 * i : 128 * (i + 1)])
        a = out[:rows]
        b = out[rows:]
        o_ref[2 * rows * i : 2 * rows * i + rows, :] = jnp.where(left, a, swap(b)).astype(bf16)
        o_ref[2 * rows * i + rows : 2 * rows * (i + 1), :] = jnp.where(left, swap(a), b).astype(bf16)


def sum_kernel(x_ref, o_ref):
    total = jnp.zeros(o_ref.shape, f32)
    rows = o_ref.shape[0]
    for i in range(x_ref.shape[0] // rows):
        total = total + x_ref[rows * i : rows * (i + 1), :].astype(f32)
    o_ref[...] = total.astype(bf16)


def combine_kernel(x_ref, u_ref, routes_ref, rw_ref, o_ref):
    rows = x_ref.shape[0]
    seqs = u_ref.shape[0]
    tables = slot_table(routes_ref, rows // 2, rows)
    x = x_ref[...]
    picked = tn(tables[0].astype(bf16), x[:, :64]) + tn(tables[1].astype(bf16), x[:, 64:])
    out = u_ref[...].astype(f32) + (
        rw_ref[:, 0:1] * picked[:seqs] + rw_ref[:, 1:2] * picked[seqs:]
    )
    o_ref[...] = out.astype(bf16)


def call(body, out, specs, scratch=(), name=None):
    return pl.pallas_call(
        body,
        out_shape=out,
        in_specs=specs,
        out_specs=jax.tree.map(lambda _: VMEM, out),
        scratch_shapes=scratch,
        compiler_params=pltpu.CompilerParams(vmem_limit_bytes=16 * 1024 * 1024),
        name=name,
    )


def sds(shape, dtype=bf16):
    return jax.ShapeDtypeStruct(shape, dtype)


def gather(x, axis):
    n = lax.axis_size(axis)
    copies = jnp.broadcast_to(x, (n, *x.shape))
    out = lax.all_to_all(copies, axis, split_axis=0, concat_axis=0, tiled=True)
    return out.reshape(n * x.shape[0], x.shape[1])


def exchange(x, axis):
    n = lax.axis_size(axis)
    rows, lanes = x.shape
    out = lax.all_to_all(
        x.reshape(n, rows // n, lanes), axis, split_axis=0, concat_axis=0, tiled=True
    )
    return out.reshape(rows, lanes)


def local(
    resid, cache_key, cache_value, lengths, lambdas, mix_gain, query_gain, key_gain, sub_gain,
    ffn_gain, w_query, w_key, w_value, w_out, routes, route_weights, w_gate, w_up, w_down,
):
    routes_t = routes.T
    packed = call(pack_kernel, sds((16, 128)), [VMEM], name="pack")(resid)
    everyone = gather(packed, "tp")
    qkv = call(
        qkv_kernel, sds((64, 128)), [VMEM] * 5, [pltpu.VMEM((64, 128), f32)], name="qkv"
    )(everyone, mix_gain.reshape(16, 128), w_query.T, w_key.T, w_value.T)
    mine = exchange(qkv, "tp")
    mixed, new_key, new_value = call(
        attend_kernel,
        (sds((8, 256)), sds((8, 256)), sds((8, 256))),
        [SMEM, SMEM] + [VMEM] * 6,
        [pltpu.VMEM((64, 128), f32), pltpu.VMEM((3, 16, 128), f32)],
        name="attend",
    )(
        lengths, lambdas, mine, cache_key[0], cache_value[0],
        query_gain.reshape(1, 128), key_gain.reshape(1, 128), sub_gain.reshape(1, 256),
    )
    heads = gather(mixed, "tp")
    updated, send = call(
        project_kernel,
        (sds((32, 64)), sds((64, 128))),
        [VMEM] * 4,
        [pltpu.VMEM((2, 256, 128), f32)],
        name="project",
    )(heads, w_out.T, resid, routes_t)
    slots = exchange(send, "ep")
    slot_rows = gather(slots, "tp")
    partial = call(expert_kernel, sds((2048, 128)), [VMEM] * 5, name="expert")(
        slot_rows, ffn_gain.reshape(16, 128), w_gate[0], w_up[0], w_down[0]
    )
    arrived = exchange(partial, "tp")
    summed = call(sum_kernel, sds((64, 128)), [VMEM], name="sum")(arrived)
    returned = exchange(summed, "ep")
    result = call(combine_kernel, sds((32, 64)), [VMEM] * 4, name="combine")(
        returned, updated, routes_t, route_weights
    )
    return (result, new_key[None], new_value[None])


def solution(mesh):
    in_specs = (
        P("ep", "tp"),
        P(("ep", "tp"), None, None, None),
        P(("ep", "tp"), None, None, None),
        P(("ep", "tp")),
        P(), P(), P(), P(), P(), P(),
        P(None, "tp"),
        P(None, "tp"),
        P(None, "tp"),
        P(None, "tp"),
        P("ep", None),
        P("ep", None),
        P("ep", None, "tp"),
        P("ep", None, "tp"),
        P("ep", "tp", None),
    )
    out_specs = (P("ep", "tp"), P(("ep", "tp"), None, None), P(("ep", "tp"), None, None))
    return jax.shard_map(local, mesh=mesh, in_specs=in_specs, out_specs=out_specs, check_vma=False)
```

time: 207 us -> 153 us (0.74)
  waiting for transfers between devices: 76 us -> 19.7 us
  blocking collectives: 60.2 us -> 107 us
  starting transfers between devices: 39.1 us -> 11.1 us
  local copies, waits for them, and re-layouts: 21.1 us -> 6.85 us
  Pallas kernels: 0 us -> 6.54 us
  other arithmetic: 4.67 us -> 0 us
  matrix products: 3.55 us -> 0 us
    all_to_all x8 -> x2, waiting for transfers between devices: 76 us -> 19.7 us  [exchange(): lax.all_to_all(x.reshape(n, rows // n, lanes), axis, split_axis=0, concat...]
    all_to_all x1 -> x5, blocking collectives: 60.2 us -> 107 us  [the longest x2 55.9 us: exchange(): lax.all_to_all(x.reshape(n, rows // n, lanes), axis, split_axis=0, concat...]
    all_to_all x8 -> x2, starting transfers between devices: 39.1 us -> 11.1 us  [exchange(): lax.all_to_all(x.reshape(n, rows // n, lanes), axis, split_axis=0, concat...]
    pallas_call x0 -> x7, Pallas kernels: none -> 6.54 us  [the longest x1 2.06 us: local(): call(attend_kernel, (sds((8, 256)), sds((8, 256)), sds((8, 256))), [SMEM,...]
    unnamed x48 -> x39, local copies, waits for them, and re-layouts: 12.8 us -> 6.72 us
    dot_general x11 -> x0, matrix products: 3.55 us -> none  [the longest x1 0.79 us: local(): jnp.dot(flat_combine, returned.reshape(-1, returned.shape[-1]), preferred...]
    reshape x4 -> x0, local copies, waits for them, and re-layouts: 2.28 us -> none  [the longest x2 1.48 us: cut_along(): return jnp.moveaxis(x.reshape(*before, size, -1, *after), dim, 0)]
  transfers between devices with their start and end apart: 8 -> 2, of which waited for: 8 -> 2; matrix products, arithmetic and copies ran while one was open for 2% -> 0% of each run, Pallas kernels for 0% -> 0%
where the time goes in v1:
time: 153 us; the launch traced here: 152 us
  blocking collectives  107 us (70%)
  waiting for transfers between devices  19.7 us (13%)
  starting transfers between devices  11.1 us (7%)
  local copies, waits for them, and re-layouts  6.85 us (4%)
  Pallas kernels  6.54 us (4%)
    all_to_all x2, blocking collectives, exchange(): lax.all_to_all(x.reshape(n, rows // n, lanes), axis, split_axis=0, concat...  55.9 us
    all_to_all x3, blocking collectives, gather(): out = lax.all_to_all(copies, axis, split_axis=0, concat_axis=0, tiled=True)  50.9 us
    all_to_all x2, waiting for transfers between devices, exchange(): lax.all_to_all(x.reshape(n, rows // n, lanes), axis, split_axis=0, concat...  19.7 us
    all_to_all x2, starting transfers between devices, exchange(): lax.all_to_all(x.reshape(n, rows // n, lanes), axis, split_axis=0, concat...  11.1 us
    unnamed x39, local copies, waits for them, and re-layouts  6.72 us
  transfers between devices with their start and end apart: 2, of which 2 were waited for; matrix products, arithmetic and copies ran while one was open for 0% of the time, Pallas kernels for 0%

profile of v1, /device:TPU:1, one launch (start us, length us, event | category | flops | bytes accessed | tf_op | source)
XLA Modules:
  0.0 152.4 jit_solution(17555498761690376309)
XLA Ops:
  0.7 0.8 copy-done.9
  1.5 19.6 %all_to_all.35 = bf16[32,16,128]{2,1,0:T(8,128)(2,1)S(1)} all-to-all(bf16[32,16,128]{2,1,0:T(8,128)(2,1)S(1)} %broadcast_in_dim.15), channel_id=1, replica_groups=mesh['ep'=32,'tp'=32] {'tp'}, dimensions={0} | all-to-all | bytes 262144 | tf_op jit(solution)/shard_map/all_to_all | solution.py:254
  21.2 0.9 copy-done.6
  22.1 0.9 copy-done.7
  23.1 0.7 copy-done.11
  23.8 1.2 qkv.1
  25.0 3.9 %all-to-all-start.1 = ((bf16[32,2,128]{2,1,0:T(2,128)(2,1)}), bf16[32,2,128]{2,1,0:T(2,128)(2,1)S(1)}, u32[]{:S(2)}, u32[]{:S(2)}) async-start(bf16[32,2,128]{2,1,0:T(2,128)(2,1)} %bitcast.5), calls=%async_computation.1 | async-start | bytes 32768 | tf_op jit(solution)/shard_map/all_to_all | solution.py:261
  29.5 7.8 %all-to-all-done.1 = bf16[32,2,128]{2,1,0:T(2,128)(2,1)S(1)} async-done(((bf16[32,2,128]{2,1,0:T(2,128)(2,1)}), bf16[32,2,128]{2,1,0:T(2,128)(2,1)S(1)}, u32[]{:S(2)}, u32[]{:S(2)}) %all-to-all-start.1) | async-done | bytes 16416 | tf_op jit(solution)/shard_map/all_to_all | solution.py:261
  37.4 0.7 copy-done.14
  38.0 1.2 copy-done.1
  39.2 2.1 %attend.1 = (bf16[8,256]{1,0:T(8,128)(2,1)S(1)}, bf16[8,256]{1,0:T(8,128)(2,1)}, bf16[8,256]{1,0:T(8,128)(2,1)}) custom-call(s32[1]{0:T(128)S(6)} %copy.23.len_ref, f32[8]{0:T(128)S(1)} %copy-done.15, bf16[64,128]{1,0:T(8,128)(2,1)S(1)} %bitcast.42, bf16[8,224,256]{2,1,0:T(8,128)(2,1)S(1)} %bitcast.31, bf16[8,224,256]{2,1,0:T(8,128)(2,1)S(1)} %bitcast.32, ...), custom_call_target="tpu_custom_call" | custom-call | tf_op jit(solution)/shard_map/attend/pallas_call | solution.py:278
  41.3 12.5 %all_to_all.36 = bf16[32,8,256]{2,1,0:T(8,128)(2,1)S(1)} all-to-all(bf16[32,8,256]{2,1,0:T(8,128)(2,1)S(1)} %broadcast_in_dim.16), channel_id=1, replica_groups=mesh['ep'=32,'tp'=32] {'tp'}, dimensions={0} | all-to-all | bytes 262144 | tf_op jit(solution)/shard_map/all_to_all | solution.py:254
  53.8 0.7 copy-done.13
  54.5 0.5 project.1
  55.0 35.1 %all_to_all.37 = bf16[32,2,128]{2,1,0:T(2,128)(2,1)S(1)} all-to-all(bf16[32,2,128]{2,1,0:T(2,128)(2,1)S(1)} %bitcast.44), channel_id=1, replica_groups=mesh['ep'=32,'tp'=32] {'ep'}, dimensions={0} | all-to-all | bytes 32768 | tf_op jit(solution)/shard_map/all_to_all | solution.py:261
  90.0 0.1 broadcast_in_dim.17
  90.2 18.8 %all_to_all.38 = bf16[32,64,128]{2,1,0:T(8,128)(2,1)S(1)} all-to-all(bf16[32,64,128]{2,1,0:T(8,128)(2,1)S(1)} %broadcast_in_dim.17), channel_id=1, replica_groups=mesh['ep'=32,'tp'=32] {'tp'}, dimensions={0} | all-to-all | bytes 1048576 | tf_op jit(solution)/shard_map/all_to_all | solution.py:254
  109.0 0.7 copy-done.12
  109.7 1.1 expert.1
  110.7 20.8 %all_to_all.39 = bf16[32,64,128]{2,1,0:T(8,128)(2,1)S(1)} all-to-all(bf16[32,64,128]{2,1,0:T(8,128)(2,1)S(1)} %bitcast.29), channel_id=1, replica_groups=mesh['ep'=32,'tp'=32] {'tp'}, dimensions={0} | all-to-all | bytes 1048576 | tf_op jit(solution)/shard_map/all_to_all | solution.py:261
  131.5 0.7 sum.1
  132.2 7.2 %all-to-all-start.6 = ((bf16[32,2,128]{2,1,0:T(2,128)(2,1)}), bf16[32,2,128]{2,1,0:T(2,128)(2,1)S(1)}, u32[]{:S(2)}, u32[]{:S(2)}) async-start(bf16[32,2,128]{2,1,0:T(2,128)(2,1)} %bitcast.24), calls=%async_computation.6 | async-start | bytes 32768 | tf_op jit(solution)/shard_map/all_to_all | solution.py:261
  139.5 11.9 %all-to-all-done.6 = bf16[32,2,128]{2,1,0:T(2,128)(2,1)S(1)} async-done(((bf16[32,2,128]{2,1,0:T(2,128)(2,1)}), bf16[32,2,128]{2,1,0:T(2,128)(2,1)S(1)}, u32[]{:S(2)}, u32[]{:S(2)}) %all-to-all-start.6) | async-done | bytes 16416 | tf_op jit(solution)/shard_map/all_to_all | solution.py:261
  151.4 1.0 combine.1
  (34 shorter events, 0.3 us)
Async XLA Ops:
  0.6 20.6 %copy-start.5 = (bf16[2048,64]{0,1:T(8,128)(2,1)S(1)}, bf16[2048,64]{0,1:T(8,128)(2,1)}, u32[]{:S(2)}) copy-start(bf16[2048,64]{0,1:T(8,128)(2,1)} %param.29) | copy-start | bytes 786436
  0.6 36.7 %copy-start = (bf16[1,8,224,256]{3,2,1,0:T(8,128)(2,1)S(1)}, bf16[1,8,224,256]{3,2,1,0:T(8,128)(2,1)}, u32[]{:S(2)}) copy-start(bf16[1,8,224,256]{3,2,1,0:T(8,128)(2,1)} %param.20) | copy-start | bytes 2752516
  0.7 0.8 copy-start.9
  21.2 1.0 copy-start.6
  22.1 0.9 copy-start.7
  23.1 0.7 copy-start.11
  25.0 12.4 %copy-start.16 = (f32[128]{0:T(128)S(1)}, f32[128]{0:T(128)}, u32[]{:S(2)}) copy-start(f32[128]{0:T(128)} %param.25) | copy-start | bytes 1540
  25.0 12.4 %copy-start.17 = (f32[128]{0:T(128)S(1)}, f32[128]{0:T(128)}, u32[]{:S(2)}) copy-start(f32[128]{0:T(128)} %param.26) | copy-start | bytes 1540
  25.0 12.4 %all-to-all-start.1 = ((bf16[32,2,128]{2,1,0:T(2,128)(2,1)}), bf16[32,2,128]{2,1,0:T(2,128)(2,1)S(1)}, u32[]{:S(2)}, u32[]{:S(2)}) async-start(bf16[32,2,128]{2,1,0:T(2,128)(2,1)} %bitcast.5), calls=%async_computation.1 | async-start | bytes 32768 | tf_op jit(solution)/shard_map/all_to_all | solution.py:261
  37.3 0.7 copy-start.14
  37.3 0.7 copy-start.15
  38.0 1.2 copy-start.1
  41.3 12.5 %copy-start.8 = (bf16[2048,64]{0,1:T(8,128)(2,1)S(1)}, bf16[2048,64]{0,1:T(8,128)(2,1)}, u32[]{:S(2)}) copy-start(bf16[2048,64]{0,1:T(8,128)(2,1)} %param.32) | copy-start | bytes 786436
  41.3 12.5 %copy-start.10 = (bf16[32,64]{1,0:T(8,128)(2,1)S(1)}, bf16[32,64]{1,0:T(8,128)(2,1)}, u32[]{:S(2)}) copy-start(bf16[32,64]{1,0:T(8,128)(2,1)} %r_ref.1) | copy-start | bytes 12292
  53.8 0.7 copy-start.13
  90.0 18.9 %copy-start.4 = (bf16[1,128,2048]{2,1,0:T(8,128)(2,1)S(1)}, bf16[1,128,2048]{2,1,0:T(8,128)(2,1)}, u32[]{:S(2)}) copy-start(bf16[1,128,2048]{2,1,0:T(8,128)(2,1)} %param.37) | copy-start | bytes 1572868
  90.2 18.8 %copy-start.2 = (bf16[1,2048,128]{2,1,0:T(8,128)(2,1)S(1)}, bf16[1,2048,128]{2,1,0:T(8,128)(2,1)}, u32[]{:S(2)}) copy-start(bf16[1,2048,128]{2,1,0:T(8,128)(2,1)} %param.35) | copy-start | bytes 1572868
  90.2 18.8 %copy-start.3 = (bf16[1,2048,128]{2,1,0:T(8,128)(2,1)S(1)}, bf16[1,2048,128]{2,1,0:T(8,128)(2,1)}, u32[]{:S(2)}) copy-start(bf16[1,2048,128]{2,1,0:T(8,128)(2,1)} %param.36) | copy-start | bytes 1572868
  109.0 0.7 copy-start.12
  132.2 7.2 %copy-start.18 = (f32[32,2]{0,1:T(2,128)S(1)}, f32[32,2]{0,1:T(2,128)}, u32[]{:S(2)}) copy-start(f32[32,2]{0,1:T(2,128)} %param.34) | copy-start | bytes 772
  132.2 19.2 %all-to-all-start.6 = ((bf16[32,2,128]{2,1,0:T(2,128)(2,1)}), bf16[32,2,128]{2,1,0:T(2,128)(2,1)S(1)}, u32[]{:S(2)}, u32[]{:S(2)}) async-start(bf16[32,2,128]{2,1,0:T(2,128)(2,1)} %bitcast.24), calls=%async_computation.6 | async-start | bytes 32768 | tf_op jit(solution)/shard_map/all_to_all | solution.py:261

commit v2 on v1

--- a/solution.py
+++ b/solution.py
@@ -17,6 +17,7 @@
 
 VMEM = pl.BlockSpec(memory_space=pltpu.VMEM)
 SMEM = pl.BlockSpec(memory_space=pltpu.SMEM)
+HBM = pl.BlockSpec(memory_space=pltpu.HBM)
 
 
 def nt(a, b):
@@ -41,10 +42,61 @@
 
 def pack_kernel(x_ref, o_ref):
     x = x_ref[...].astype(f32)
-    o_ref[...] = jnp.concatenate([x[:16], x[16:]], axis=1).astype(bf16)
-
-
-def qkv_kernel(x_ref, gain_ref, wq_ref, wk_ref, wv_ref, o_ref, s_ref):
+    packed = jnp.concatenate([x[:16], x[16:]], axis=1).astype(bf16)
+    for i in range(o_ref.shape[0] // 16):
+        o_ref[16 * i : 16 * (i + 1), :] = packed
+
+
+def as_column(row):
+    n = row.shape[1]
+    eye = lax.broadcasted_iota(jnp.int32, (n, n), 0) == lax.broadcasted_iota(jnp.int32, (n, n), 1)
+    return jnp.sum(jnp.where(eye, row, 0.0), axis=1, keepdims=True)
+
+
+def stage_kernel(*refs):
+    n = (len(refs) - 8) // 2
+    len_ref, lam_ref, routes_ref, rw_ref = refs[:4]
+    sources, targets = refs[4 : 4 + n], refs[4 + n : 2 + 2 * n]
+    disp_ref, comb_ref, w_ref, lamcol_ref, live_ref, sems = refs[2 + 2 * n :]
+    width = sources[0].shape[0]
+    targets = [targets[0].at[width * i : width * (i + 1), :] for i in range(3)] + list(targets[1:])
+    copies = [
+        pltpu.make_async_copy(src, dst, sems.at[i]) for i, (src, dst) in enumerate(zip(sources, targets))
+    ]
+    for c in copies:
+        c.start()
+    experts = disp_ref.shape[1] // 2
+    rows = disp_ref.shape[1]
+    hit_row = jnp.concatenate([routes_ref[0:1, :], routes_ref[1:2, :]], axis=1)
+    pairs = hit_row.shape[1]
+    seqs = pairs // 2
+    hit = (lax.broadcasted_iota(jnp.int32, (experts, pairs), 0) == hit_row).astype(f32)
+    upper = (
+        lax.broadcasted_iota(jnp.int32, (pairs, pairs), 0)
+        < lax.broadcasted_iota(jnp.int32, (pairs, pairs), 1)
+    ).astype(bf16)
+    before = nn(hit.astype(bf16), upper)
+    slot_row = jnp.sum(before * hit, axis=0, keepdims=True)
+    slot = slot_row.astype(jnp.int32)
+    place = hit_row * 2 + slot // 2
+    half = slot % 2
+    at = lax.broadcasted_iota(jnp.int32, (rows, pairs), 0) == place
+    place_col = as_column(place.astype(f32)).astype(jnp.int32)
+    half_col = as_column(half.astype(f32)).astype(jnp.int32)
+    at_col = lax.broadcasted_iota(jnp.int32, (pairs, rows), 1) == place_col
+    for j in (0, 1):
+        table = (at & (half == j)).astype(f32)
+        disp_ref[j] = (table[:, :seqs] + table[:, seqs:]).astype(bf16)
+        comb_ref[j] = (at_col & (half_col == j)).astype(bf16)
+    w_row = jnp.concatenate([rw_ref[0:1, :], rw_ref[1:2, :]], axis=1)
+    w_ref[...] = jnp.broadcast_to(as_column(w_row), w_ref.shape)
+    lamcol_ref[...] = jnp.broadcast_to(as_column(lam_ref[...]), lamcol_ref.shape)
+    live_ref[...] = jnp.full(live_ref.shape, len_ref[0], jnp.int32)
+    for c in copies:
+        c.wait()
+
+
+def qkv_kernel(x_ref, gain_ref, w_ref, o_ref, s_ref):
     tp = x_ref.shape[0] // 16
     left = left_half((16, 128))
     tiles = []
@@ -63,17 +115,19 @@
         [(tile * scale * gain_ref[i : i + 1, :]).astype(bf16) for i, tile in enumerate(tiles)],
         axis=1,
     )
-    q = nt(normed, wq_ref[...])
-    k = nt(normed, wk_ref[...])
-    v = nt(normed, wv_ref[...])
-    s_ref[pl.ds(0, 32, stride=2), :] = jnp.concatenate([q, k], axis=1)
+    out = nt(normed, w_ref[...])
+    v = out[:, 128:192]
+    s_ref[pl.ds(0, 32, stride=2), :] = out[:, :128]
     s_ref[pl.ds(1, 32, stride=2), :] = jnp.concatenate([v, jnp.zeros_like(v)], axis=1)
     o_ref[...] = s_ref[...].astype(bf16)
 
 
 def attend_kernel(
-    len_ref, lam_ref, x_ref, ck_ref, cv_ref, qg_ref, kg_ref, sg_ref, o_ref, nk_ref, nv_ref, s_ref, p_ref
+    live_ref, lam_ref, x_ref, ck_ref, cv_hbm, qg_ref, kg_ref, sg_ref, o_ref, nk_ref, nv_ref,
+    s_ref, p_ref, cv_ref, sem,
 ):
+    values = pltpu.make_async_copy(cv_hbm, cv_ref, sem)
+    values.start()
     heads, length, width = ck_ref.shape
     s_ref[...] = x_ref[...].astype(f32)
     rows = 2 * heads
@@ -115,7 +169,7 @@
     scale = 128.0 ** -0.5
     scores = scores * scale
     own = jnp.sum(qu * ku, axis=1, keepdims=True) * scale
-    live = lax.broadcasted_iota(jnp.int32, (rows, length), 1) < len_ref[0]
+    live = lax.broadcasted_iota(jnp.int32, (rows, length), 1) < live_ref[:, 0:1]
     scores = jnp.where(live, scores, MASKED)
     peak = jnp.maximum(jnp.max(scores, axis=1, keepdims=True), own)
     weight = jnp.exp(scores - peak)
@@ -126,9 +180,7 @@
     p_ref[1] = jnp.concatenate([prob[:, 128:length], jnp.zeros((rows, 256 - length), f32)], axis=1)
     p_ref[2] = jnp.broadcast_to(own_weight / totals, (rows, 128))
     head = lax.broadcasted_iota(jnp.int32, (heads, 1), 0)
-    lam = jnp.zeros((heads, 1), f32)
-    for h in range(heads):
-        lam = jnp.where(head == h, lam_ref[h], lam)
+    lam = lam_ref[...]
     mixes = [
         p_ref[pl.ds(j, 1), pl.ds(0, heads, stride=2), :][0] - lam * p_ref[pl.ds(j, 1), pl.ds(1, heads, stride=2), :][0]
         for j in range(3)
@@ -136,29 +188,17 @@
     past_mix = jnp.concatenate(mixes[:2], axis=1)[:, 0:length]
     own_mix = mixes[2][:, 0:1].astype(bf16).astype(f32)
     out = own_mix * new_value.astype(bf16).astype(f32)
+    values.wait()
     for h in range(heads):
         lhs = jnp.where(head == h, past_mix, 0.0).astype(bf16)
         out = out + nn(lhs, cv_ref[h])
     r = lax.rsqrt(jnp.mean(out * out, axis=1, keepdims=True) + EPS)
-    o_ref[...] = (out * r * sg_ref[...] * OUT_FACTOR).astype(bf16)
-
-
-def slot_table(routes_ref, experts, rows):
-    hit_row = jnp.concatenate([routes_ref[0:1, :], routes_ref[1:2, :]], axis=1)
-    pairs = hit_row.shape[1]
-    hit = (lax.broadcasted_iota(jnp.int32, (experts, pairs), 0) == hit_row).astype(f32)
-    upper = (
-        lax.broadcasted_iota(jnp.int32, (pairs, pairs), 0)
-        < lax.broadcasted_iota(jnp.int32, (pairs, pairs), 1)
-    ).astype(bf16)
-    before = nn(hit.astype(bf16), upper)
-    slot = jnp.sum(before * hit, axis=0, keepdims=True).astype(jnp.int32)
-    place = hit_row * 2 + slot // 2
-    at = lax.broadcasted_iota(jnp.int32, (rows, pairs), 0) == place
-    return [(at & (slot % 2 == half)).astype(f32) for half in (0, 1)]
-
-
-def project_kernel(x_ref, w_ref, r_ref, routes_ref, u_ref, o_ref, s_ref):
+    mixed = (out * r * sg_ref[...] * OUT_FACTOR).astype(bf16)
+    for i in range(o_ref.shape[0] // heads):
+        o_ref[heads * i : heads * (i + 1), :] = mixed
+
+
+def project_kernel(x_ref, w_ref, r_ref, disp_ref, u_ref, o_ref, s_ref):
     seqs = r_ref.shape[0]
     heads = x_ref.shape[0] // seqs
     width = x_ref.shape[1]
@@ -176,9 +216,7 @@
     acc = acc + nt(mixed, w_ref[...])
     updated = acc.astype(bf16)
     u_ref[...] = updated
-    rows = o_ref.shape[0]
-    tables = slot_table(routes_ref, rows // 2, rows)
-    halves = [nn((t[:, :seqs] + t[:, seqs:]).astype(bf16), updated) for t in tables]
+    halves = [nn(disp_ref[j], updated) for j in (0, 1)]
     o_ref[...] = jnp.concatenate(halves, axis=1).astype(bf16)
 
 
@@ -220,15 +258,12 @@
     o_ref[...] = total.astype(bf16)
 
 
-def combine_kernel(x_ref, u_ref, routes_ref, rw_ref, o_ref):
-    rows = x_ref.shape[0]
+def combine_kernel(x_ref, u_ref, comb_ref, w_ref, o_ref):
     seqs = u_ref.shape[0]
-    tables = slot_table(routes_ref, rows // 2, rows)
     x = x_ref[...]
-    picked = tn(tables[0].astype(bf16), x[:, :64]) + tn(tables[1].astype(bf16), x[:, 64:])
-    out = u_ref[...].astype(f32) + (
-        rw_ref[:, 0:1] * picked[:seqs] + rw_ref[:, 1:2] * picked[seqs:]
-    )
+    picked = nn(comb_ref[0], x[:, :64]) + nn(comb_ref[1], x[:, 64:])
+    picked = picked * w_ref[:, :64]
+    out = u_ref[...].astype(f32) + (picked[:seqs] + picked[seqs:])
     o_ref[...] = out.astype(bf16)
 
 
@@ -239,7 +274,7 @@
         in_specs=specs,
         out_specs=jax.tree.map(lambda _: VMEM, out),
         scratch_shapes=scratch,
-        compiler_params=pltpu.CompilerParams(vmem_limit_bytes=16 * 1024 * 1024),
+        compiler_params=pltpu.CompilerParams(vmem_limit_bytes=8 * 1024 * 1024),
         name=name,
     )
 
@@ -248,11 +283,9 @@
     return jax.ShapeDtypeStruct(shape, dtype)
 
 
-def gather(x, axis):
+def broadcast(x, axis):
     n = lax.axis_size(axis)
-    copies = jnp.broadcast_to(x, (n, *x.shape))
-    out = lax.all_to_all(copies, axis, split_axis=0, concat_axis=0, tiled=True)
-    return out.reshape(n * x.shape[0], x.shape[1])
+    return jnp.broadcast_to(x, (n, *x.shape)).reshape(n * x.shape[0], x.shape[1])
 
 
 def exchange(x, axis):
@@ -268,41 +301,60 @@
     resid, cache_key, cache_value, lengths, lambdas, mix_gain, query_gain, key_gain, sub_gain,
     ffn_gain, w_query, w_key, w_value, w_out, routes, route_weights, w_gate, w_up, w_down,
 ):
-    routes_t = routes.T
-    packed = call(pack_kernel, sds((16, 128)), [VMEM], name="pack")(resid)
-    everyone = gather(packed, "tp")
+    packed = call(pack_kernel, sds((512, 128)), [VMEM], name="pack")(resid)
+    everyone = exchange(packed, "tp")
+    staged = [
+        w_query.T, w_key.T, w_value.T, mix_gain.reshape(16, 128),
+        cache_key[0],
+        query_gain.reshape(1, 128), key_gain.reshape(1, 128), sub_gain.reshape(1, 256),
+        w_out.T, resid, ffn_gain.reshape(16, 128),
+    ]
+    tables = (
+        sds((2, 64, 32)), sds((2, 64, 64)), sds((64, 128), f32),
+        sds((8, 128), f32), sds((16, 128), jnp.int32),
+    )
+    out = call(
+        stage_kernel,
+        (sds((192, 2048)),) + tuple(sds(a.shape, a.dtype) for a in staged[3:]) + tables,
+        [SMEM, VMEM, VMEM, VMEM] + [HBM] * len(staged),
+        [pltpu.SemaphoreType.DMA((len(staged),))],
+        name="stage",
+    )(lengths, lambdas.reshape(1, 8), routes.T, route_weights.T, *staged)
+    wqkv, mg, ck, qg, kg, sg, wo, own, fg, disp, comb, rw, lam, live = out
     qkv = call(
-        qkv_kernel, sds((64, 128)), [VMEM] * 5, [pltpu.VMEM((64, 128), f32)], name="qkv"
-    )(everyone, mix_gain.reshape(16, 128), w_query.T, w_key.T, w_value.T)
+        qkv_kernel, sds((64, 128)), [VMEM] * 3, [pltpu.VMEM((64, 128), f32)], name="qkv"
+    )(everyone, mg, wqkv)
     mine = exchange(qkv, "tp")
     mixed, new_key, new_value = call(
         attend_kernel,
-        (sds((8, 256)), sds((8, 256)), sds((8, 256))),
-        [SMEM, SMEM] + [VMEM] * 6,
-        [pltpu.VMEM((64, 128), f32), pltpu.VMEM((3, 16, 128), f32)],
+        (sds((256, 256)), sds((8, 256)), sds((8, 256))),
+        [VMEM, VMEM, VMEM, VMEM, HBM, VMEM, VMEM, VMEM],
+        [
+            pltpu.VMEM((64, 128), f32),
+            pltpu.VMEM((3, 16, 128), f32),
+            pltpu.VMEM(cache_value.shape[1:], bf16),
+            pltpu.SemaphoreType.DMA,
+        ],
         name="attend",
-    )(
-        lengths, lambdas, mine, cache_key[0], cache_value[0],
-        query_gain.reshape(1, 128), key_gain.reshape(1, 128), sub_gain.reshape(1, 256),
-    )
-    heads = gather(mixed, "tp")
+    )(live, lam, mine, ck, cache_value[0], qg, kg, sg)
+    heads = exchange(mixed, "tp")
     updated, send = call(
         project_kernel,
         (sds((32, 64)), sds((64, 128))),
         [VMEM] * 4,
         [pltpu.VMEM((2, 256, 128), f32)],
         name="project",
-    )(heads, w_out.T, resid, routes_t)
+    )(heads, wo, own, disp)
     slots = exchange(send, "ep")
-    slot_rows = gather(slots, "tp")
+    slot_rows = exchange(broadcast(slots, "tp"), "tp")
     partial = call(expert_kernel, sds((2048, 128)), [VMEM] * 5, name="expert")(
-        slot_rows, ffn_gain.reshape(16, 128), w_gate[0], w_up[0], w_down[0]
+        slot_rows, fg, w_gate[0], w_up[0], w_down[0]
     )
     arrived = exchange(partial, "tp")
     summed = call(sum_kernel, sds((64, 128)), [VMEM], name="sum")(arrived)
     returned = exchange(summed, "ep")
     result = call(combine_kernel, sds((32, 64)), [VMEM] * 4, name="combine")(
-        returned, updated, routes_t, route_weights
+        returned, updated, comb, rw
     )
     return (result, new_key[None], new_value[None])
 

time: 153 us -> 146 us (0.954)
  waiting for transfers between devices: 19.7 us -> 3.09 us
  blocking collectives: 107 us -> 119 us
    all_to_all x2 -> x6, blocking collectives: 55.9 us -> 119 us  [exchange(): lax.all_to_all(x.reshape(n, rows // n, lanes), axis, split_axis=0, concat...]
    all_to_all x3 -> x0, blocking collectives: 50.9 us -> none  [gather(): out = lax.all_to_all(copies, axis, split_axis=0, concat_axis=0, tiled=True)]
    all_to_all x2 -> x1, waiting for transfers between devices: 19.7 us -> 3.09 us  [exchange(): lax.all_to_all(x.reshape(n, rows // n, lanes), axis, split_axis=0, concat...]
    unnamed x39 -> x38, local copies, waits for them, and re-layouts: 6.72 us -> 5.45 us
    all_to_all x2 -> x1, starting transfers between devices: 11.1 us -> 10.6 us  [exchange(): lax.all_to_all(x.reshape(n, rows // n, lanes), axis, split_axis=0, concat...]
    pallas_call x3 -> x4, Pallas kernels: 3.32 us -> 3.73 us  [the longest x1 1.67 us: local(): call(attend_kernel, (sds((256, 256)), sds((8, 256)), sds((8, 256))), [VME...]
  transfers between devices with their start and end apart: 2 -> 1, of which waited for: 2 -> 1; matrix products, arithmetic and copies ran while one was open for 0% -> 0% of each run, Pallas kernels for 0% -> 1%
where the time goes in v2:
time: 146 us
  blocking collectives  119 us (82%)
  starting transfers between devices  10.6 us (7%)
  Pallas kernels  6.07 us (4%)
  local copies, waits for them, and re-layouts  5.56 us (4%)
  waiting for transfers between devices  3.09 us (2%)
  between operations  1.47 us (1%)
    all_to_all x6, blocking collectives, exchange(): lax.all_to_all(x.reshape(n, rows // n, lanes), axis, split_axis=0, concat...  119 us
    all_to_all x1, starting transfers between devices, exchange(): lax.all_to_all(x.reshape(n, rows // n, lanes), axis, split_axis=0, concat...  10.6 us
    unnamed x38, local copies, waits for them, and re-layouts  5.45 us
    all_to_all x1, waiting for transfers between devices, exchange(): lax.all_to_all(x.reshape(n, rows // n, lanes), axis, split_axis=0, concat...  3.09 us
  transfers between devices with their start and end apart: 1, of which 1 were waited for; matrix products, arithmetic and copies ran while one was open for 0% of the time, Pallas kernels for 1%

profile of v2, /device:TPU:1, one launch (start us, length us, event | category | flops | bytes accessed | tf_op | source)
XLA Modules:
  0.0 145.8 jit_solution(5489461029855875973)
XLA Ops:
  0.7 0.7 copy-done.9
  1.4 0.7 pack.1
  2.1 10.6 %all-to-all-start = ((bf16[32,16,128]{2,1,0:T(8,128)(2,1)}), bf16[32,16,128]{2,1,0:T(8,128)(2,1)S(1)}, u32[]{:S(2)}, u32[]{:S(2)}) async-start(bf16[32,16,128]{2,1,0:T(8,128)(2,1)} %bitcast.13), calls=%async_computation | async-start | bytes 262144 | tf_op jit(solution)/shard_map/all_to_all | solution.py:294
  13.5 0.6 copy-done.12
  14.1 0.0 copy-done.11
  14.2 1.2 copy-done
  15.3 0.9 copy-done.6
  16.3 0.9 copy-done.7
  17.2 0.9 copy-done.8
  18.2 0.8 stage.1
  19.0 3.1 %all-to-all-done = bf16[32,16,128]{2,1,0:T(8,128)(2,1)S(1)} async-done(((bf16[32,16,128]{2,1,0:T(8,128)(2,1)}), bf16[32,16,128]{2,1,0:T(8,128)(2,1)S(1)}, u32[]{:S(2)}, u32[]{:S(2)}) %all-to-all-start) | async-done | bytes 131104 | tf_op jit(solution)/shard_map/all_to_all | solution.py:294
  22.1 0.5 qkv.1
  22.6 14.5 %all_to_all.35 = bf16[32,2,128]{2,1,0:T(2,128)(2,1)S(1)} all-to-all(bf16[32,2,128]{2,1,0:T(2,128)(2,1)S(1)} %bitcast.48), channel_id=1, replica_groups=mesh['ep'=32,'tp'=32] {'tp'}, dimensions={0} | all-to-all | bytes 32768 | tf_op jit(solution)/shard_map/all_to_all | solution.py:294
  37.2 1.7 %attend.1 = (bf16[256,256]{1,0:T(8,128)(2,1)S(1)}, bf16[8,256]{1,0:T(8,128)(2,1)}, bf16[8,256]{1,0:T(8,128)(2,1)}) custom-call(s32[16,128]{1,0:T(8,128)S(1)} %get-tuple-element.22.live_ref, f32[8,128]{1,0:T(8,128)S(1)} %get-tuple-element.23.lam_ref, bf16[64,128]{1,0:T(8,128)(2,1)S(1)} %bitcast.47, bf16[8,224,256]{2,1,0:T(8,128)(2,1)S(1)} %get-tuple-element.26.ck_ref, ...), custom_call_target="tpu_custom_call" | custom-call | tf_op jit(solution)/shard_map/attend/pallas_call | solution.py:328
  38.9 12.4 %all_to_all.36 = bf16[32,8,256]{2,1,0:T(8,128)(2,1)S(1)} all-to-all(bf16[32,8,256]{2,1,0:T(8,128)(2,1)S(1)} %bitcast.46), channel_id=1, replica_groups=mesh['ep'=32,'tp'=32] {'tp'}, dimensions={0} | all-to-all | bytes 262144 | tf_op jit(solution)/shard_map/all_to_all | solution.py:294
  51.3 0.4 project.1
  51.6 34.4 %all_to_all.37 = bf16[32,2,128]{2,1,0:T(2,128)(2,1)S(1)} all-to-all(bf16[32,2,128]{2,1,0:T(2,128)(2,1)S(1)} %bitcast.51), channel_id=1, replica_groups=mesh['ep'=32,'tp'=32] {'ep'}, dimensions={0} | all-to-all | bytes 32768 | tf_op jit(solution)/shard_map/all_to_all | solution.py:294
  86.0 0.1 broadcast_in_dim.9
  86.1 18.8 %all_to_all.38 = bf16[32,64,128]{2,1,0:T(8,128)(2,1)S(1)} all-to-all(bf16[32,64,128]{2,1,0:T(8,128)(2,1)S(1)} %broadcast_in_dim.9), channel_id=1, replica_groups=mesh['ep'=32,'tp'=32] {'tp'}, dimensions={0} | all-to-all | bytes 1048576 | tf_op jit(solution)/shard_map/all_to_all | solution.py:294
  104.9 1.1 expert.1
  106.0 20.8 %all_to_all.39 = bf16[32,64,128]{2,1,0:T(8,128)(2,1)S(1)} all-to-all(bf16[32,64,128]{2,1,0:T(8,128)(2,1)S(1)} %bitcast.33), channel_id=1, replica_groups=mesh['ep'=32,'tp'=32] {'tp'}, dimensions={0} | all-to-all | bytes 1048576 | tf_op jit(solution)/shard_map/all_to_all | solution.py:294
  126.8 0.1 sum.1
  126.9 18.2 %all_to_all.40 = bf16[32,2,128]{2,1,0:T(2,128)(2,1)S(1)} all-to-all(bf16[32,2,128]{2,1,0:T(2,128)(2,1)S(1)} %bitcast.49), channel_id=1, replica_groups=mesh['ep'=32,'tp'=32] {'ep'}, dimensions={0} | all-to-all | bytes 32768 | tf_op jit(solution)/shard_map/all_to_all | solution.py:294
  145.0 0.8 combine.1
  (31 shorter events, 0.1 us)
Async XLA Ops:
  0.6 12.8 %copy-start.5 = (bf16[2048,64]{0,1:T(8,128)(2,1)S(1)}, bf16[2048,64]{0,1:T(8,128)(2,1)}, u32[]{:S(2)}) copy-start(bf16[2048,64]{0,1:T(8,128)(2,1)} %param.29) | copy-start | bytes 786436
  0.6 0.7 copy-start.9
  2.1 11.4 %copy-start.13 = (s32[32,2]{0,1:T(2,128)S(1)}, s32[32,2]{0,1:T(2,128)}, u32[]{:S(2)}) copy-start(s32[32,2]{0,1:T(2,128)} %param.33) | copy-start | bytes 772
  2.1 11.4 %copy-start.14 = (f32[32,2]{0,1:T(2,128)S(1)}, f32[32,2]{0,1:T(2,128)}, u32[]{:S(2)}) copy-start(f32[32,2]{0,1:T(2,128)} %param.34) | copy-start | bytes 772
  2.1 11.4 %copy-start.15 = (f32[256]{0:T(256)S(1)}, f32[256]{0:T(256)}, u32[]{:S(2)}) copy-start(f32[256]{0:T(256)} %param.27) | copy-start | bytes 3076
  2.1 11.4 %copy-start.17 = (f32[128]{0:T(128)S(1)}, f32[128]{0:T(128)}, u32[]{:S(2)}) copy-start(f32[128]{0:T(128)} %param.25) | copy-start | bytes 1540
  2.1 11.4 %copy-start.18 = (f32[128]{0:T(128)S(1)}, f32[128]{0:T(128)}, u32[]{:S(2)}) copy-start(f32[128]{0:T(128)} %param.26) | copy-start | bytes 1540
  2.1 20.0 %all-to-all-start = ((bf16[32,16,128]{2,1,0:T(8,128)(2,1)}), bf16[32,16,128]{2,1,0:T(8,128)(2,1)S(1)}, u32[]{:S(2)}, u32[]{:S(2)}) async-start(bf16[32,16,128]{2,1,0:T(8,128)(2,1)} %bitcast.13), calls=%async_computation | async-start | bytes 262144 | tf_op jit(solution)/shard_map/all_to_all | solution.py:294
  13.4 0.7 copy-start.12
  13.4 0.7 copy-start.11
  13.4 0.7 copy-start.10
  13.5 0.7 copy-start.16
  14.2 1.2 copy-start
  15.3 0.9 copy-start.6
  16.3 0.9 copy-start.7
  17.2 0.9 copy-start.8
  19.0 18.2 %copy-start.1 = (bf16[1,8,224,256]{3,2,1,0:T(8,128)(2,1)S(1)}, bf16[1,8,224,256]{3,2,1,0:T(8,128)(2,1)}, u32[]{:S(2)}) copy-start(bf16[1,8,224,256]{3,2,1,0:T(8,128)(2,1)} %param.21) | copy-start | bytes 2752516
  86.0 18.9 %copy-start.4 = (bf16[1,128,2048]{2,1,0:T(8,128)(2,1)S(1)}, bf16[1,128,2048]{2,1,0:T(8,128)(2,1)}, u32[]{:S(2)}) copy-start(bf16[1,128,2048]{2,1,0:T(8,128)(2,1)} %param.37) | copy-start | bytes 1572868
  86.1 18.8 %copy-start.2 = (bf16[1,2048,128]{2,1,0:T(8,128)(2,1)S(1)}, bf16[1,2048,128]{2,1,0:T(8,128)(2,1)}, u32[]{:S(2)}) copy-start(bf16[1,2048,128]{2,1,0:T(8,128)(2,1)} %param.35) | copy-start | bytes 1572868
  86.1 18.8 %copy-start.3 = (bf16[1,2048,128]{2,1,0:T(8,128)(2,1)S(1)}, bf16[1,2048,128]{2,1,0:T(8,128)(2,1)}, u32[]{:S(2)}) copy-start(bf16[1,2048,128]{2,1,0:T(8,128)(2,1)} %param.36) | copy-start | bytes 1572868

commit v3 on v2

--- a/solution.py
+++ b/solution.py
@@ -40,7 +40,24 @@
     return pltpu.roll(x, 64, 1)
 
 
-def pack_kernel(x_ref, o_ref):
+MIX, FFN, QG, KG, SG, LAM, LENGTH, ROUTES, WEIGHTS, SMALL = 0, 16, 32, 33, 34, 36, 37, 38, 40, 48
+
+
+def lead_kernel(len_ref, o_ref):
+    o_ref[...] = jnp.full(o_ref.shape, len_ref[0], jnp.int32).astype(f32)
+
+
+def pack_kernel(x_ref, mix_ref, ffn_ref, qg_ref, kg_ref, sg_ref, lam_ref, len_ref, routes_ref, rw_ref, o_ref, small_ref):
+    small_ref[...] = jnp.zeros(small_ref.shape, f32)
+    small_ref[MIX:FFN, :] = mix_ref[...]
+    small_ref[FFN:QG, :] = ffn_ref[...]
+    small_ref[QG : QG + 1, :] = qg_ref[...]
+    small_ref[KG : KG + 1, :] = kg_ref[...]
+    small_ref[SG : SG + 2, :] = sg_ref[...]
+    small_ref[LAM : LAM + 1, 0 : lam_ref.shape[1]] = lam_ref[...]
+    small_ref[LENGTH : LENGTH + 1, :] = len_ref[0:1, :]
+    small_ref[ROUTES : ROUTES + 2, 0 : routes_ref.shape[1]] = routes_ref[...].astype(f32)
+    small_ref[WEIGHTS : WEIGHTS + 2, 0 : rw_ref.shape[1]] = rw_ref[...]
     x = x_ref[...].astype(f32)
     packed = jnp.concatenate([x[:16], x[16:]], axis=1).astype(bf16)
     for i in range(o_ref.shape[0] // 16):
@@ -53,50 +70,24 @@
     return jnp.sum(jnp.where(eye, row, 0.0), axis=1, keepdims=True)
 
 
-def stage_kernel(*refs):
-    n = (len(refs) - 8) // 2
-    len_ref, lam_ref, routes_ref, rw_ref = refs[:4]
-    sources, targets = refs[4 : 4 + n], refs[4 + n : 2 + 2 * n]
-    disp_ref, comb_ref, w_ref, lamcol_ref, live_ref, sems = refs[2 + 2 * n :]
-    width = sources[0].shape[0]
-    targets = [targets[0].at[width * i : width * (i + 1), :] for i in range(3)] + list(targets[1:])
-    copies = [
-        pltpu.make_async_copy(src, dst, sems.at[i]) for i, (src, dst) in enumerate(zip(sources, targets))
-    ]
-    for c in copies:
-        c.start()
-    experts = disp_ref.shape[1] // 2
-    rows = disp_ref.shape[1]
-    hit_row = jnp.concatenate([routes_ref[0:1, :], routes_ref[1:2, :]], axis=1)
+def pair_row(small_ref, at, seqs):
+    return jnp.concatenate([small_ref[at : at + 1, 0:seqs], small_ref[at + 1 : at + 2, 0:seqs]], axis=1)
+
+
+def slots_of(small_ref, experts, seqs):
+    hit_row = pair_row(small_ref, ROUTES, seqs).astype(jnp.int32)
     pairs = hit_row.shape[1]
-    seqs = pairs // 2
     hit = (lax.broadcasted_iota(jnp.int32, (experts, pairs), 0) == hit_row).astype(f32)
     upper = (
         lax.broadcasted_iota(jnp.int32, (pairs, pairs), 0)
         < lax.broadcasted_iota(jnp.int32, (pairs, pairs), 1)
     ).astype(bf16)
     before = nn(hit.astype(bf16), upper)
-    slot_row = jnp.sum(before * hit, axis=0, keepdims=True)
-    slot = slot_row.astype(jnp.int32)
-    place = hit_row * 2 + slot // 2
-    half = slot % 2
-    at = lax.broadcasted_iota(jnp.int32, (rows, pairs), 0) == place
-    place_col = as_column(place.astype(f32)).astype(jnp.int32)
-    half_col = as_column(half.astype(f32)).astype(jnp.int32)
-    at_col = lax.broadcasted_iota(jnp.int32, (pairs, rows), 1) == place_col
-    for j in (0, 1):
-        table = (at & (half == j)).astype(f32)
-        disp_ref[j] = (table[:, :seqs] + table[:, seqs:]).astype(bf16)
-        comb_ref[j] = (at_col & (half_col == j)).astype(bf16)
-    w_row = jnp.concatenate([rw_ref[0:1, :], rw_ref[1:2, :]], axis=1)
-    w_ref[...] = jnp.broadcast_to(as_column(w_row), w_ref.shape)
-    lamcol_ref[...] = jnp.broadcast_to(as_column(lam_ref[...]), lamcol_ref.shape)
-    live_ref[...] = jnp.full(live_ref.shape, len_ref[0], jnp.int32)
-    for c in copies:
-        c.wait()
-
-
-def qkv_kernel(x_ref, gain_ref, w_ref, o_ref, s_ref):
+    slot = jnp.sum(before * hit, axis=0, keepdims=True).astype(jnp.int32)
+    return hit_row * 2 + slot // 2, slot % 2
+
+
+def qkv_kernel(x_ref, small_ref, wq_ref, wk_ref, wv_ref, o_ref, s_ref):
     tp = x_ref.shape[0] // 16
     left = left_half((16, 128))
     tiles = []
@@ -112,10 +103,11 @@
     width = 64.0 * tp
     scale = lax.rsqrt(jnp.sum(total, axis=1, keepdims=True) / width + EPS)
     normed = jnp.concatenate(
-        [(tile * scale * gain_ref[i : i + 1, :]).astype(bf16) for i, tile in enumerate(tiles)],
+        [(tile * scale * small_ref[MIX + i : MIX + i + 1, :]).astype(bf16) for i, tile in enumerate(tiles)],
         axis=1,
     )
-    out = nt(normed, w_ref[...])
+    w = jnp.concatenate([wq_ref[...], wk_ref[...], wv_ref[...]], axis=0)
+    out = nt(normed, w)
     v = out[:, 128:192]
     s_ref[pl.ds(0, 32, stride=2), :] = out[:, :128]
     s_ref[pl.ds(1, 32, stride=2), :] = jnp.concatenate([v, jnp.zeros_like(v)], axis=1)
@@ -123,11 +115,9 @@
 
 
 def attend_kernel(
-    live_ref, lam_ref, x_ref, ck_ref, cv_hbm, qg_ref, kg_ref, sg_ref, o_ref, nk_ref, nv_ref,
-    s_ref, p_ref, cv_ref, sem,
+    x_ref, small_ref, ck_ref, cv_ref, o_ref, nk_ref, nv_ref,
+    s_ref, p_ref,
 ):
-    values = pltpu.make_async_copy(cv_hbm, cv_ref, sem)
-    values.start()
     heads, length, width = ck_ref.shape
     s_ref[...] = x_ref[...].astype(f32)
     rows = 2 * heads
@@ -144,8 +134,8 @@
         r = lax.rsqrt(jnp.mean(z * z, axis=1, keepdims=True) + EPS)
         return (z * r * gain).astype(bf16).astype(f32)
 
-    qu = unit(q, qg_ref[...])
-    ku = unit(k, kg_ref[...])
+    qu = unit(q, small_ref[QG : QG + 1, :])
+    ku = unit(k, small_ref[KG : KG + 1, :])
     s_ref[0:rows, :] = ku
     s_ref[rows : 2 * rows, :] = v
     new_key = jnp.concatenate(
@@ -169,7 +159,7 @@
     scale = 128.0 ** -0.5
     scores = scores * scale
     own = jnp.sum(qu * ku, axis=1, keepdims=True) * scale
-    live = lax.broadcasted_iota(jnp.int32, (rows, length), 1) < live_ref[:, 0:1]
+    live = lax.broadcasted_iota(jnp.int32, (rows, length), 1) < small_ref[LENGTH : LENGTH + 1, 0:1].astype(jnp.int32)
     scores = jnp.where(live, scores, MASKED)
     peak = jnp.maximum(jnp.max(scores, axis=1, keepdims=True), own)
     weight = jnp.exp(scores - peak)
@@ -180,7 +170,7 @@
     p_ref[1] = jnp.concatenate([prob[:, 128:length], jnp.zeros((rows, 256 - length), f32)], axis=1)
     p_ref[2] = jnp.broadcast_to(own_weight / totals, (rows, 128))
     head = lax.broadcasted_iota(jnp.int32, (heads, 1), 0)
-    lam = lam_ref[...]
+    lam = as_column(small_ref[LAM : LAM + 1, 0:heads])
     mixes = [
         p_ref[pl.ds(j, 1), pl.ds(0, heads, stride=2), :][0] - lam * p_ref[pl.ds(j, 1), pl.ds(1, heads, stride=2), :][0]
         for j in range(3)
@@ -188,17 +178,17 @@
     past_mix = jnp.concatenate(mixes[:2], axis=1)[:, 0:length]
     own_mix = mixes[2][:, 0:1].astype(bf16).astype(f32)
     out = own_mix * new_value.astype(bf16).astype(f32)
-    values.wait()
     for h in range(heads):
         lhs = jnp.where(head == h, past_mix, 0.0).astype(bf16)
         out = out + nn(lhs, cv_ref[h])
     r = lax.rsqrt(jnp.mean(out * out, axis=1, keepdims=True) + EPS)
-    mixed = (out * r * sg_ref[...] * OUT_FACTOR).astype(bf16)
+    sub = jnp.concatenate([small_ref[SG : SG + 1, :], small_ref[SG + 1 : SG + 2, :]], axis=1)
+    mixed = (out * r * sub * OUT_FACTOR).astype(bf16)
     for i in range(o_ref.shape[0] // heads):
         o_ref[heads * i : heads * (i + 1), :] = mixed
 
 
-def project_kernel(x_ref, w_ref, r_ref, disp_ref, u_ref, o_ref, s_ref):
+def project_kernel(x_ref, w_ref, r_ref, small_ref, u_ref, o_ref, s_ref):
     seqs = r_ref.shape[0]
     heads = x_ref.shape[0] // seqs
     width = x_ref.shape[1]
@@ -216,11 +206,15 @@
     acc = acc + nt(mixed, w_ref[...])
     updated = acc.astype(bf16)
     u_ref[...] = updated
-    halves = [nn(disp_ref[j], updated) for j in (0, 1)]
+    rows = o_ref.shape[0]
+    place, half = slots_of(small_ref, rows // 2, seqs)
+    at = lax.broadcasted_iota(jnp.int32, (rows, 2 * seqs), 0) == place
+    tables = [(at & (half == j)).astype(f32) for j in (0, 1)]
+    halves = [nn((t[:, :seqs] + t[:, seqs:]).astype(bf16), updated) for t in tables]
     o_ref[...] = jnp.concatenate(halves, axis=1).astype(bf16)
 
 
-def expert_kernel(x_ref, gain_ref, wg_ref, wu_ref, wd_ref, o_ref):
+def expert_kernel(x_ref, small_ref, wg_ref, wu_ref, wd_ref, o_ref):
     rows = 64
     tp = x_ref.shape[0] // rows
     left = left_half((rows, 128))
@@ -236,7 +230,7 @@
         tiles.append(tile)
     scale = lax.rsqrt(jnp.sum(total, axis=1, keepdims=True) / (64.0 * tp) + EPS)
     hidden = jnp.concatenate(
-        [(tile * scale * gain_ref[i : i + 1, :]).astype(bf16) for i, tile in enumerate(tiles)],
+        [(tile * scale * small_ref[FFN + i : FFN + i + 1, :]).astype(bf16) for i, tile in enumerate(tiles)],
         axis=1,
     )
     gate = nn(hidden, wg_ref[...])
@@ -258,16 +252,22 @@
     o_ref[...] = total.astype(bf16)
 
 
-def combine_kernel(x_ref, u_ref, comb_ref, w_ref, o_ref):
+def combine_kernel(x_ref, u_ref, small_ref, o_ref):
     seqs = u_ref.shape[0]
+    rows = x_ref.shape[0]
+    place, half = slots_of(small_ref, rows // 2, seqs)
+    place_col = as_column(place.astype(f32)).astype(jnp.int32)
+    half_col = as_column(half.astype(f32)).astype(jnp.int32)
+    at = lax.broadcasted_iota(jnp.int32, (2 * seqs, rows), 1) == place_col
+    tables = [(at & (half_col == j)).astype(bf16) for j in (0, 1)]
     x = x_ref[...]
-    picked = nn(comb_ref[0], x[:, :64]) + nn(comb_ref[1], x[:, 64:])
-    picked = picked * w_ref[:, :64]
+    picked = nn(tables[0], x[:, :64]) + nn(tables[1], x[:, 64:])
+    picked = picked * as_column(pair_row(small_ref, WEIGHTS, seqs))
     out = u_ref[...].astype(f32) + (picked[:seqs] + picked[seqs:])
     o_ref[...] = out.astype(bf16)
 
 
-def call(body, out, specs, scratch=(), name=None):
+def call(body, out, specs, scratch=(), name=None, flops=None):
     return pl.pallas_call(
         body,
         out_shape=out,
@@ -276,6 +276,7 @@
         scratch_shapes=scratch,
         compiler_params=pltpu.CompilerParams(vmem_limit_bytes=8 * 1024 * 1024),
         name=name,
+        cost_estimate=flops and pl.CostEstimate(flops=flops, bytes_accessed=0, transcendentals=0),
     )
 
 
@@ -301,42 +302,30 @@
     resid, cache_key, cache_value, lengths, lambdas, mix_gain, query_gain, key_gain, sub_gain,
     ffn_gain, w_query, w_key, w_value, w_out, routes, route_weights, w_gate, w_up, w_down,
 ):
-    packed = call(pack_kernel, sds((512, 128)), [VMEM], name="pack")(resid)
+    length = call(lead_kernel, sds((8, 128), f32), [SMEM], name="lead", flops=3000000000)(lengths)
+    packed, small = call(
+        pack_kernel, (sds((512, 128)), sds((SMALL, 128), f32)), [VMEM] * 10, name="pack", flops=3000000000
+    )(
+        resid, mix_gain.reshape(16, 128), ffn_gain.reshape(16, 128), query_gain.reshape(1, 128),
+        key_gain.reshape(1, 128), sub_gain.reshape(2, 128), lambdas.reshape(1, 8),
+        length, routes.T, route_weights.T,
+    )
     everyone = exchange(packed, "tp")
-    staged = [
-        w_query.T, w_key.T, w_value.T, mix_gain.reshape(16, 128),
-        cache_key[0],
-        query_gain.reshape(1, 128), key_gain.reshape(1, 128), sub_gain.reshape(1, 256),
-        w_out.T, resid, ffn_gain.reshape(16, 128),
-    ]
-    tables = (
-        sds((2, 64, 32)), sds((2, 64, 64)), sds((64, 128), f32),
-        sds((8, 128), f32), sds((16, 128), jnp.int32),
-    )
-    out = call(
-        stage_kernel,
-        (sds((192, 2048)),) + tuple(sds(a.shape, a.dtype) for a in staged[3:]) + tables,
-        [SMEM, VMEM, VMEM, VMEM] + [HBM] * len(staged),
-        [pltpu.SemaphoreType.DMA((len(staged),))],
-        name="stage",
-    )(lengths, lambdas.reshape(1, 8), routes.T, route_weights.T, *staged)
-    wqkv, mg, ck, qg, kg, sg, wo, own, fg, disp, comb, rw, lam, live = out
     qkv = call(
-        qkv_kernel, sds((64, 128)), [VMEM] * 3, [pltpu.VMEM((64, 128), f32)], name="qkv"
-    )(everyone, mg, wqkv)
+        qkv_kernel, sds((64, 128)), [VMEM] * 5, [pltpu.VMEM((64, 128), f32)], name="qkv", flops=3000000000
+    )(everyone, small, w_query.T, w_key.T, w_value.T)
     mine = exchange(qkv, "tp")
     mixed, new_key, new_value = call(
         attend_kernel,
         (sds((256, 256)), sds((8, 256)), sds((8, 256))),
-        [VMEM, VMEM, VMEM, VMEM, HBM, VMEM, VMEM, VMEM],
+        [VMEM] * 4,
         [
             pltpu.VMEM((64, 128), f32),
             pltpu.VMEM((3, 16, 128), f32),
-            pltpu.VMEM(cache_value.shape[1:], bf16),
-            pltpu.SemaphoreType.DMA,
         ],
         name="attend",
-    )(live, lam, mine, ck, cache_value[0], qg, kg, sg)
+        flops=3000000000,
+    )(mine, small, cache_key[0], cache_value[0])
     heads = exchange(mixed, "tp")
     updated, send = call(
         project_kernel,
@@ -344,17 +333,18 @@
         [VMEM] * 4,
         [pltpu.VMEM((2, 256, 128), f32)],
         name="project",
-    )(heads, wo, own, disp)
+        flops=3000000000,
+    )(heads, w_out.T, resid, small)
     slots = exchange(send, "ep")
     slot_rows = exchange(broadcast(slots, "tp"), "tp")
-    partial = call(expert_kernel, sds((2048, 128)), [VMEM] * 5, name="expert")(
-        slot_rows, fg, w_gate[0], w_up[0], w_down[0]
+    partial = call(expert_kernel, sds((2048, 128)), [VMEM] * 5, name="expert", flops=3000000000)(
+        slot_rows, small, w_gate[0], w_up[0], w_down[0]
     )
     arrived = exchange(partial, "tp")
-    summed = call(sum_kernel, sds((64, 128)), [VMEM], name="sum")(arrived)
+    summed = call(sum_kernel, sds((64, 128)), [VMEM], name="sum", flops=3000000000)(arrived)
     returned = exchange(summed, "ep")
-    result = call(combine_kernel, sds((32, 64)), [VMEM] * 4, name="combine")(
-        returned, updated, comb, rw
+    result = call(combine_kernel, sds((32, 64)), [VMEM] * 3, name="combine")(
+        returned, updated, small
     )
     return (result, new_key[None], new_value[None])
 

time: 146 us -> 145 us (level)
  blocking collectives: 119 us -> 137 us
  starting transfers between devices: 10.6 us -> 0 us
  local copies, waits for them, and re-layouts: 5.56 us -> 0.87 us
  waiting for transfers between devices: 3.09 us -> 0 us
    all_to_all x6 -> x7, blocking collectives: 119 us -> 137 us  [exchange(): lax.all_to_all(x.reshape(n, rows // n, lanes), axis, split_axis=0, concat...]
    all_to_all x1 -> x0, starting transfers between devices: 10.6 us -> none  [exchange(): lax.all_to_all(x.reshape(n, rows // n, lanes), axis, split_axis=0, concat...]
    unnamed x38 -> x36, local copies, waits for them, and re-layouts: 5.45 us -> 0.76 us
    all_to_all x1 -> x0, waiting for transfers between devices: 3.09 us -> none  [exchange(): lax.all_to_all(x.reshape(n, rows // n, lanes), axis, split_axis=0, concat...]
  transfers between devices with their start and end apart: 1 -> 0, of which waited for: 1 -> 0; matrix products, arithmetic and copies ran while one was open for 0% -> 0% of each run, Pallas kernels for 1% -> 0%
where the time goes in v3:
time: 145 us; the launch traced here: 144 us
  blocking collectives  137 us (94%)
  Pallas kernels  4.81 us (3%)
  between operations  1.46 us (1%)
    all_to_all x7, blocking collectives, exchange(): lax.all_to_all(x.reshape(n, rows // n, lanes), axis, split_axis=0, concat...  137 us

profile of v3, /device:TPU:1, one launch (start us, length us, event | category | flops | bytes accessed | tf_op | source)
XLA Modules:
  0.0 144.1 jit_solution(2422972652863256517)
XLA Ops:
  1.4 0.0 copy-start.15
  1.4 0.6 copy-done.10
  2.0 0.0 copy-done.11
  2.0 0.0 copy-done.14
  2.0 0.0 copy-done.17
  2.0 0.1 copy-done.9
  2.1 0.1 pack.1
  2.2 0.0 copy-start.5
  2.2 19.8 %all_to_all.35 = bf16[32,16,128]{2,1,0:T(8,128)(2,1)S(1)} all-to-all(bf16[32,16,128]{2,1,0:T(8,128)(2,1)S(1)} %bitcast.36), channel_id=1, replica_groups=mesh['ep'=32,'tp'=32] {'tp'}, dimensions={0} | all-to-all | bytes 262144 | tf_op jit(solution)/shard_map/all_to_all | solution.py:295
  22.0 0.0 copy-start
  22.0 0.0 copy-start.1
  22.0 0.5 qkv.1
  22.5 11.6 %all_to_all.36 = bf16[32,2,128]{2,1,0:T(2,128)(2,1)S(1)} all-to-all(bf16[32,2,128]{2,1,0:T(2,128)(2,1)S(1)} %bitcast.42), channel_id=1, replica_groups=mesh['ep'=32,'tp'=32] {'tp'}, dimensions={0} | all-to-all | bytes 32768 | tf_op jit(solution)/shard_map/all_to_all | solution.py:295
  34.1 1.5 %attend.1 = (bf16[256,256]{1,0:T(8,128)(2,1)S(1)}, bf16[8,256]{1,0:T(8,128)(2,1)}, bf16[8,256]{1,0:T(8,128)(2,1)}) custom-call(bf16[64,128]{1,0:T(8,128)(2,1)S(1)} %bitcast.40, f32[48,128]{1,0:T(8,128)S(1)} %get-tuple-element.11.small_ref, bf16[8,224,256]{2,1,0:T(8,128)(2,1)S(1)} %bitcast.44, bf16[8,224,256]{2,1,0:T(8,128)(2,1)S(1)} %bitcast.45), custom_call_target="tpu_custom_call" | custom-call | flops 3000000000 | tf_op jit(solution)/shard_map/attend/pallas_call | solution.py:318
  35.7 12.5 %all_to_all.37 = bf16[32,8,256]{2,1,0:T(8,128)(2,1)S(1)} all-to-all(bf16[32,8,256]{2,1,0:T(8,128)(2,1)S(1)} %bitcast.35), channel_id=1, replica_groups=mesh['ep'=32,'tp'=32] {'tp'}, dimensions={0} | all-to-all | bytes 262144 | tf_op jit(solution)/shard_map/all_to_all | solution.py:295
  48.2 0.5 project.1
  48.7 35.3 %all_to_all.38 = bf16[32,2,128]{2,1,0:T(2,128)(2,1)S(1)} all-to-all(bf16[32,2,128]{2,1,0:T(2,128)(2,1)S(1)} %bitcast.41), channel_id=1, replica_groups=mesh['ep'=32,'tp'=32] {'ep'}, dimensions={0} | all-to-all | bytes 32768 | tf_op jit(solution)/shard_map/all_to_all | solution.py:295
  84.0 0.1 broadcast_in_dim.9
  84.1 18.8 %all_to_all.39 = bf16[32,64,128]{2,1,0:T(8,128)(2,1)S(1)} all-to-all(bf16[32,64,128]{2,1,0:T(8,128)(2,1)S(1)} %broadcast_in_dim.9), channel_id=1, replica_groups=mesh['ep'=32,'tp'=32] {'tp'}, dimensions={0} | all-to-all | bytes 1048576 | tf_op jit(solution)/shard_map/all_to_all | solution.py:295
  102.9 1.1 expert.1
  104.0 20.8 %all_to_all.40 = bf16[32,64,128]{2,1,0:T(8,128)(2,1)S(1)} all-to-all(bf16[32,64,128]{2,1,0:T(8,128)(2,1)S(1)} %bitcast.33), channel_id=1, replica_groups=mesh['ep'=32,'tp'=32] {'tp'}, dimensions={0} | all-to-all | bytes 1048576 | tf_op jit(solution)/shard_map/all_to_all | solution.py:295
  124.8 0.1 sum.1
  124.9 18.1 %all_to_all.41 = bf16[32,2,128]{2,1,0:T(2,128)(2,1)S(1)} all-to-all(bf16[32,2,128]{2,1,0:T(2,128)(2,1)S(1)} %bitcast.43), channel_id=1, replica_groups=mesh['ep'=32,'tp'=32] {'ep'}, dimensions={0} | all-to-all | bytes 32768 | tf_op jit(solution)/shard_map/all_to_all | solution.py:295
  143.0 1.0 combine.1
  (28 shorter events, 0.1 us)
Async XLA Ops:
  1.3 0.7 copy-start.10
  1.3 0.7 copy-start.11
  1.3 0.7 copy-start.13
  1.3 0.7 copy-start.14
  1.3 0.7 copy-start.16
  1.3 0.7 copy-start.17
  1.3 0.7 copy-start.9
  1.4 0.7 copy-start.12
  1.4 0.7 copy-start.15
  2.1 19.9 %copy-start.6 = (bf16[2048,64]{0,1:T(8,128)(2,1)S(1)}, bf16[2048,64]{0,1:T(8,128)(2,1)}, u32[]{:S(2)}) copy-start(bf16[2048,64]{0,1:T(8,128)(2,1)} %param.30) | copy-start | bytes 786436
  2.1 19.9 %copy-start.7 = (bf16[2048,64]{0,1:T(8,128)(2,1)S(1)}, bf16[2048,64]{0,1:T(8,128)(2,1)}, u32[]{:S(2)}) copy-start(bf16[2048,64]{0,1:T(8,128)(2,1)} %param.31) | copy-start | bytes 786436
  2.2 19.8 %copy-start.5 = (bf16[2048,64]{0,1:T(8,128)(2,1)S(1)}, bf16[2048,64]{0,1:T(8,128)(2,1)}, u32[]{:S(2)}) copy-start(bf16[2048,64]{0,1:T(8,128)(2,1)} %param.29) | copy-start | bytes 786436
  22.0 12.2 %copy-start = (bf16[1,8,224,256]{3,2,1,0:T(8,128)(2,1)S(1)}, bf16[1,8,224,256]{3,2,1,0:T(8,128)(2,1)}, u32[]{:S(2)}) copy-start(bf16[1,8,224,256]{3,2,1,0:T(8,128)(2,1)} %param.20) | copy-start | bytes 2752516
  22.0 12.2 %copy-start.1 = (bf16[1,8,224,256]{3,2,1,0:T(8,128)(2,1)S(1)}, bf16[1,8,224,256]{3,2,1,0:T(8,128)(2,1)}, u32[]{:S(2)}) copy-start(bf16[1,8,224,256]{3,2,1,0:T(8,128)(2,1)} %param.21) | copy-start | bytes 2752516
  35.7 12.5 %copy-start.8 = (bf16[2048,64]{0,1:T(8,128)(2,1)S(1)}, bf16[2048,64]{0,1:T(8,128)(2,1)}, u32[]{:S(2)}) copy-start(bf16[2048,64]{0,1:T(8,128)(2,1)} %param.32) | copy-start | bytes 786436
  48.6 54.3 %copy-start.4 = (bf16[1,128,2048]{2,1,0:T(8,128)(2,1)S(1)}, bf16[1,128,2048]{2,1,0:T(8,128)(2,1)}, u32[]{:S(2)}) copy-start(bf16[1,128,2048]{2,1,0:T(8,128)(2,1)} %param.37) | copy-start | bytes 1572868
  84.1 18.8 %copy-start.2 = (bf16[1,2048,128]{2,1,0:T(8,128)(2,1)S(1)}, bf16[1,2048,128]{2,1,0:T(8,128)(2,1)}, u32[]{:S(2)}) copy-start(bf16[1,2048,128]{2,1,0:T(8,128)(2,1)} %param.35) | copy-start | bytes 1572868
  84.1 18.8 %copy-start.3 = (bf16[1,2048,128]{2,1,0:T(8,128)(2,1)S(1)}, bf16[1,2048,128]{2,1,0:T(8,128)(2,1)}, u32[]{:S(2)}) copy-start(bf16[1,2048,128]{2,1,0:T(8,128)(2,1)} %param.36) | copy-start | bytes 1572868

commit v4 on v3

--- a/solution.py
+++ b/solution.py
@@ -85,6 +85,21 @@
     before = nn(hit.astype(bf16), upper)
     slot = jnp.sum(before * hit, axis=0, keepdims=True).astype(jnp.int32)
     return hit_row * 2 + slot // 2, slot % 2
+
+
+def route_tables(small_ref, disp_ref, comb_ref, w_ref):
+    rows = disp_ref.shape[1]
+    seqs = disp_ref.shape[2]
+    place, half = slots_of(small_ref, rows // 2, seqs)
+    at = lax.broadcasted_iota(jnp.int32, (rows, 2 * seqs), 0) == place
+    place_col = as_column(place.astype(f32)).astype(jnp.int32)
+    half_col = as_column(half.astype(f32)).astype(jnp.int32)
+    at_col = lax.broadcasted_iota(jnp.int32, (2 * seqs, rows), 1) == place_col
+    for j in (0, 1):
+        table = (at & (half == j)).astype(f32)
+        disp_ref[j] = (table[:, :seqs] + table[:, seqs:]).astype(bf16)
+        comb_ref[j] = (at_col & (half_col == j)).astype(bf16)
+    w_ref[...] = jnp.broadcast_to(as_column(pair_row(small_ref, WEIGHTS, seqs)), w_ref.shape)
 
 
 def qkv_kernel(x_ref, small_ref, wq_ref, wk_ref, wv_ref, o_ref, s_ref):
@@ -115,7 +130,7 @@
 
 
 def attend_kernel(
-    x_ref, small_ref, ck_ref, cv_ref, o_ref, nk_ref, nv_ref,
+    x_ref, small_ref, ck_ref, cv_ref, o_ref, nk_ref, nv_ref, disp_ref, comb_ref, w_ref,
     s_ref, p_ref,
 ):
     heads, length, width = ck_ref.shape
@@ -184,11 +199,12 @@
     r = lax.rsqrt(jnp.mean(out * out, axis=1, keepdims=True) + EPS)
     sub = jnp.concatenate([small_ref[SG : SG + 1, :], small_ref[SG + 1 : SG + 2, :]], axis=1)
     mixed = (out * r * sub * OUT_FACTOR).astype(bf16)
+    route_tables(small_ref, disp_ref, comb_ref, w_ref)
     for i in range(o_ref.shape[0] // heads):
         o_ref[heads * i : heads * (i + 1), :] = mixed
 
 
-def project_kernel(x_ref, w_ref, r_ref, small_ref, u_ref, o_ref, s_ref):
+def project_kernel(x_ref, w_ref, r_ref, disp_ref, u_ref, o_ref, s_ref):
     seqs = r_ref.shape[0]
     heads = x_ref.shape[0] // seqs
     width = x_ref.shape[1]
@@ -206,11 +222,7 @@
     acc = acc + nt(mixed, w_ref[...])
     updated = acc.astype(bf16)
     u_ref[...] = updated
-    rows = o_ref.shape[0]
-    place, half = slots_of(small_ref, rows // 2, seqs)
-    at = lax.broadcasted_iota(jnp.int32, (rows, 2 * seqs), 0) == place
-    tables = [(at & (half == j)).astype(f32) for j in (0, 1)]
-    halves = [nn((t[:, :seqs] + t[:, seqs:]).astype(bf16), updated) for t in tables]
+    halves = [nn(disp_ref[j], updated) for j in (0, 1)]
     o_ref[...] = jnp.concatenate(halves, axis=1).astype(bf16)
 
 
@@ -218,30 +230,36 @@
     rows = 64
     tp = x_ref.shape[0] // rows
     left = left_half((rows, 128))
+    left_row = left_half((1, 128))
+    total = jnp.zeros((rows, 128), f32)
+    for i in range(tp):
+        x = x_ref[rows * i : rows * (i + 1), :].astype(f32)
+        total = total + x * x
+    sums = [jnp.sum(jnp.where(left == keep, total, 0.0), axis=1, keepdims=True) for keep in (True, False)]
+    scales = [lax.rsqrt(v / (64.0 * tp) + EPS) for v in sums]
+    scale = jnp.where(left, scales[0], scales[1])
     tiles = []
-    total = jnp.zeros((2 * rows, 128), f32)
     for i in range(tp // 2):
-        a = x_ref[2 * rows * i : 2 * rows * i + rows, :].astype(f32)
-        b = x_ref[2 * rows * i + rows : 2 * rows * (i + 1), :].astype(f32)
-        tile = jnp.concatenate(
-            [jnp.where(left, a, swap(b)), jnp.where(left, swap(a), b)], axis=0
-        )
-        total = total + tile * tile
-        tiles.append(tile)
-    scale = lax.rsqrt(jnp.sum(total, axis=1, keepdims=True) / (64.0 * tp) + EPS)
-    hidden = jnp.concatenate(
-        [(tile * scale * small_ref[FFN + i : FFN + i + 1, :]).astype(bf16) for i, tile in enumerate(tiles)],
-        axis=1,
-    )
-    gate = nn(hidden, wg_ref[...])
-    up = nn(hidden, wu_ref[...])
-    act = (gate / (1.0 + jnp.exp(-gate)) * up).astype(bf16)
+        gain = small_ref[FFN + i : FFN + i + 1, :]
+        turned = swap(gain)
+        gains = (jnp.where(left_row, gain, turned), jnp.where(left_row, turned, gain))
+        a, b = [
+            (x_ref[rows * (2 * i + j) : rows * (2 * i + j + 1), :].astype(f32) * scale * gains[j]).astype(bf16)
+            for j in (0, 1)
+        ]
+        tiles.append(jnp.concatenate([jnp.where(left, a, swap(b)), jnp.where(left, swap(a), b)], axis=0))
+    hidden = jnp.concatenate(tiles, axis=1)
+    both = nn(hidden, jnp.concatenate([wg_ref[...], wu_ref[...]], axis=1))
+    gate = both[:, :128]
+    act = (gate / (1.0 + jnp.exp(-gate)) * both[:, 128:]).astype(bf16)
     for i in range(tp // 2):
-        out = nn(act, wd_ref[:, 128 * i : 128 * (i + 1)])
+        if i % 2 == 0:
+            pair = nn(act, wd_ref[:, 128 * i : 128 * (i + 2)])
+        out = pair[:, 128 * (i % 2) : 128 * (i % 2 + 1)].astype(bf16)
         a = out[:rows]
         b = out[rows:]
-        o_ref[2 * rows * i : 2 * rows * i + rows, :] = jnp.where(left, a, swap(b)).astype(bf16)
-        o_ref[2 * rows * i + rows : 2 * rows * (i + 1), :] = jnp.where(left, swap(a), b).astype(bf16)
+        o_ref[2 * rows * i : 2 * rows * i + rows, :] = jnp.where(left, a, swap(b))
+        o_ref[2 * rows * i + rows : 2 * rows * (i + 1), :] = jnp.where(left, swap(a), b)
 
 
 def sum_kernel(x_ref, o_ref):
@@ -252,17 +270,13 @@
     o_ref[...] = total.astype(bf16)
 
 
-def combine_kernel(x_ref, u_ref, small_ref, o_ref):
+def combine_kernel(x_ref, u_ref, comb_ref, w_ref, key_ref, value_ref, o_ref, nk_ref, nv_ref):
+    nk_ref[...] = key_ref[...]
+    nv_ref[...] = value_ref[...]
     seqs = u_ref.shape[0]
-    rows = x_ref.shape[0]
-    place, half = slots_of(small_ref, rows // 2, seqs)
-    place_col = as_column(place.astype(f32)).astype(jnp.int32)
-    half_col = as_column(half.astype(f32)).astype(jnp.int32)
-    at = lax.broadcasted_iota(jnp.int32, (2 * seqs, rows), 1) == place_col
-    tables = [(at & (half_col == j)).astype(bf16) for j in (0, 1)]
     x = x_ref[...]
-    picked = nn(tables[0], x[:, :64]) + nn(tables[1], x[:, 64:])
-    picked = picked * as_column(pair_row(small_ref, WEIGHTS, seqs))
+    picked = nn(comb_ref[0], x[:, :64]) + nn(comb_ref[1], x[:, 64:])
+    picked = picked * w_ref[:, :64]
     out = u_ref[...].astype(f32) + (picked[:seqs] + picked[seqs:])
     o_ref[...] = out.astype(bf16)
 
@@ -315,9 +329,12 @@
         qkv_kernel, sds((64, 128)), [VMEM] * 5, [pltpu.VMEM((64, 128), f32)], name="qkv", flops=3000000000
     )(everyone, small, w_query.T, w_key.T, w_value.T)
     mine = exchange(qkv, "tp")
-    mixed, new_key, new_value = call(
+    mixed, new_key, new_value, disp, comb, rw = call(
         attend_kernel,
-        (sds((256, 256)), sds((8, 256)), sds((8, 256))),
+        (
+            sds((256, 256)), sds((8, 256)), sds((8, 256)),
+            sds((2, 64, 32)), sds((2, 64, 64)), sds((64, 128), f32),
+        ),
         [VMEM] * 4,
         [
             pltpu.VMEM((64, 128), f32),
@@ -334,7 +351,7 @@
         [pltpu.VMEM((2, 256, 128), f32)],
         name="project",
         flops=3000000000,
-    )(heads, w_out.T, resid, small)
+    )(heads, w_out.T, resid, disp)
     slots = exchange(send, "ep")
     slot_rows = exchange(broadcast(slots, "tp"), "tp")
     partial = call(expert_kernel, sds((2048, 128)), [VMEM] * 5, name="expert", flops=3000000000)(
@@ -343,9 +360,9 @@
     arrived = exchange(partial, "tp")
     summed = call(sum_kernel, sds((64, 128)), [VMEM], name="sum", flops=3000000000)(arrived)
     returned = exchange(summed, "ep")
-    result = call(combine_kernel, sds((32, 64)), [VMEM] * 3, name="combine")(
-        returned, updated, small
-    )
+    result, new_key, new_value = call(
+        combine_kernel, (sds((32, 64)), sds((8, 256)), sds((8, 256))), [VMEM] * 6, name="combine"
+    )(returned, updated, comb, rw, new_key, new_value)
     return (result, new_key[None], new_value[None])
 
 

time: 145 us -> 144 us (level)
  no operation moved by 1% of the time
where the time goes in v4:
time: 144 us
  blocking collectives  137 us (95%)
  Pallas kernels  4.34 us (3%)
  between operations  1.46 us (1%)
    all_to_all x7, blocking collectives, exchange(): lax.all_to_all(x.reshape(n, rows // n, lanes), axis, split_axis=0, concat...  137 us

profile of v4, /device:TPU:1, one launch (start us, length us, event | category | flops | bytes accessed | tf_op | source)
XLA Modules:
  0.0 143.6 jit_solution(9435272290272931114)
XLA Ops:
  1.4 0.0 copy-start.12
  1.4 0.0 copy-start.15
  1.4 0.6 copy-done.10
  2.0 0.0 copy-done.11
  2.0 0.0 copy-done.14
  2.0 0.0 copy-done.17
  2.0 0.1 copy-done.9
  2.1 0.1 pack.1
  2.2 19.8 %all_to_all.35 = bf16[32,16,128]{2,1,0:T(8,128)(2,1)S(1)} all-to-all(bf16[32,16,128]{2,1,0:T(8,128)(2,1)S(1)} %bitcast.37), channel_id=1, replica_groups=mesh['ep'=32,'tp'=32] {'tp'}, dimensions={0} | all-to-all | bytes 262144 | tf_op jit(solution)/shard_map/all_to_all | solution.py:309
  22.0 0.0 copy-start
  22.0 0.5 qkv.1
  22.5 11.6 %all_to_all.36 = bf16[32,2,128]{2,1,0:T(2,128)(2,1)S(1)} all-to-all(bf16[32,2,128]{2,1,0:T(2,128)(2,1)S(1)} %bitcast.42), channel_id=1, replica_groups=mesh['ep'=32,'tp'=32] {'tp'}, dimensions={0} | all-to-all | bytes 32768 | tf_op jit(solution)/shard_map/all_to_all | solution.py:309
  34.1 1.3 attend.1
  35.4 12.5 %all_to_all.37 = bf16[32,8,256]{2,1,0:T(8,128)(2,1)S(1)} all-to-all(bf16[32,8,256]{2,1,0:T(8,128)(2,1)S(1)} %bitcast.35), channel_id=1, replica_groups=mesh['ep'=32,'tp'=32] {'tp'}, dimensions={0} | all-to-all | bytes 262144 | tf_op jit(solution)/shard_map/all_to_all | solution.py:309
  47.9 0.4 project.1
  48.3 0.0 copy-start.4
  48.4 35.3 %all_to_all.38 = bf16[32,2,128]{2,1,0:T(2,128)(2,1)S(1)} all-to-all(bf16[32,2,128]{2,1,0:T(2,128)(2,1)S(1)} %bitcast.41), channel_id=1, replica_groups=mesh['ep'=32,'tp'=32] {'ep'}, dimensions={0} | all-to-all | bytes 32768 | tf_op jit(solution)/shard_map/all_to_all | solution.py:309
  83.7 0.1 broadcast_in_dim.9
  83.8 18.8 %all_to_all.39 = bf16[32,64,128]{2,1,0:T(8,128)(2,1)S(1)} all-to-all(bf16[32,64,128]{2,1,0:T(8,128)(2,1)S(1)} %broadcast_in_dim.9), channel_id=1, replica_groups=mesh['ep'=32,'tp'=32] {'tp'}, dimensions={0} | all-to-all | bytes 1048576 | tf_op jit(solution)/shard_map/all_to_all | solution.py:309
  102.6 1.2 expert.1
  103.8 20.8 %all_to_all.40 = bf16[32,64,128]{2,1,0:T(8,128)(2,1)S(1)} all-to-all(bf16[32,64,128]{2,1,0:T(8,128)(2,1)S(1)} %bitcast.33), channel_id=1, replica_groups=mesh['ep'=32,'tp'=32] {'tp'}, dimensions={0} | all-to-all | bytes 1048576 | tf_op jit(solution)/shard_map/all_to_all | solution.py:309
  124.6 0.1 sum.1
  124.7 18.1 %all_to_all.41 = bf16[32,2,128]{2,1,0:T(2,128)(2,1)S(1)} all-to-all(bf16[32,2,128]{2,1,0:T(2,128)(2,1)S(1)} %bitcast.43), channel_id=1, replica_groups=mesh['ep'=32,'tp'=32] {'ep'}, dimensions={0} | all-to-all | bytes 32768 | tf_op jit(solution)/shard_map/all_to_all | solution.py:309
  142.8 0.8 combine.1
  (28 shorter events, 0.1 us)
Async XLA Ops:
  1.3 0.7 copy-start.10
  1.3 0.7 copy-start.11
  1.3 0.7 copy-start.13
  1.3 0.7 copy-start.14
  1.3 0.7 copy-start.16
  1.3 0.7 copy-start.17
  1.3 0.7 copy-start.9
  1.4 0.7 copy-start.12
  1.4 0.7 copy-start.15
  2.1 19.9 %copy-start.6 = (bf16[2048,64]{0,1:T(8,128)(2,1)S(1)}, bf16[2048,64]{0,1:T(8,128)(2,1)}, u32[]{:S(2)}) copy-start(bf16[2048,64]{0,1:T(8,128)(2,1)} %param.30) | copy-start | bytes 786436
  2.1 19.9 %copy-start.7 = (bf16[2048,64]{0,1:T(8,128)(2,1)S(1)}, bf16[2048,64]{0,1:T(8,128)(2,1)}, u32[]{:S(2)}) copy-start(bf16[2048,64]{0,1:T(8,128)(2,1)} %param.31) | copy-start | bytes 786436
  2.2 19.8 %copy-start.5 = (bf16[2048,64]{0,1:T(8,128)(2,1)S(1)}, bf16[2048,64]{0,1:T(8,128)(2,1)}, u32[]{:S(2)}) copy-start(bf16[2048,64]{0,1:T(8,128)(2,1)} %param.29) | copy-start | bytes 786436
  22.0 12.2 %copy-start = (bf16[1,8,224,256]{3,2,1,0:T(8,128)(2,1)S(1)}, bf16[1,8,224,256]{3,2,1,0:T(8,128)(2,1)}, u32[]{:S(2)}) copy-start(bf16[1,8,224,256]{3,2,1,0:T(8,128)(2,1)} %param.20) | copy-start | bytes 2752516
  22.0 12.2 %copy-start.1 = (bf16[1,8,224,256]{3,2,1,0:T(8,128)(2,1)S(1)}, bf16[1,8,224,256]{3,2,1,0:T(8,128)(2,1)}, u32[]{:S(2)}) copy-start(bf16[1,8,224,256]{3,2,1,0:T(8,128)(2,1)} %param.21) | copy-start | bytes 2752516
  35.4 12.5 %copy-start.8 = (bf16[2048,64]{0,1:T(8,128)(2,1)S(1)}, bf16[2048,64]{0,1:T(8,128)(2,1)}, u32[]{:S(2)}) copy-start(bf16[2048,64]{0,1:T(8,128)(2,1)} %param.32) | copy-start | bytes 786436
  48.3 54.3 %copy-start.4 = (bf16[1,128,2048]{2,1,0:T(8,128)(2,1)S(1)}, bf16[1,128,2048]{2,1,0:T(8,128)(2,1)}, u32[]{:S(2)}) copy-start(bf16[1,128,2048]{2,1,0:T(8,128)(2,1)} %param.37) | copy-start | bytes 1572868
  83.8 18.8 %copy-start.2 = (bf16[1,2048,128]{2,1,0:T(8,128)(2,1)S(1)}, bf16[1,2048,128]{2,1,0:T(8,128)(2,1)}, u32[]{:S(2)}) copy-start(bf16[1,2048,128]{2,1,0:T(8,128)(2,1)} %param.35) | copy-start | bytes 1572868
  83.8 18.8 %copy-start.3 = (bf16[1,2048,128]{2,1,0:T(8,128)(2,1)S(1)}, bf16[1,2048,128]{2,1,0:T(8,128)(2,1)}, u32[]{:S(2)}) copy-start(bf16[1,2048,128]{2,1,0:T(8,128)(2,1)} %param.36) | copy-start | bytes 1572868

commit v5 on v4

--- a/solution.py
+++ b/solution.py
@@ -102,27 +102,35 @@
     w_ref[...] = jnp.broadcast_to(as_column(pair_row(small_ref, WEIGHTS, seqs)), w_ref.shape)
 
 
+def normed_rows(x_ref, small_ref, at, rows, tp):
+    left = left_half((rows, 128))
+    left_row = left_half((1, 128))
+    total = jnp.zeros((rows, 128), f32)
+    for i in range(tp):
+        x = x_ref[rows * i : rows * (i + 1), :].astype(f32)
+        total = total + x * x
+    sums = [jnp.sum(jnp.where(left == keep, total, 0.0), axis=1, keepdims=True) for keep in (True, False)]
+    scales = [lax.rsqrt(v / (64.0 * tp) + EPS) for v in sums]
+    scale = jnp.where(left, scales[0], scales[1])
+    tiles = []
+    for i in range(tp // 2):
+        gain = small_ref[at + i : at + i + 1, :]
+        turned = swap(gain)
+        gains = (jnp.where(left_row, gain, turned), jnp.where(left_row, turned, gain))
+        a, b = [
+            (x_ref[rows * (2 * i + j) : rows * (2 * i + j + 1), :].astype(f32) * scale * gains[j]).astype(bf16)
+            for j in (0, 1)
+        ]
+        tiles.append(jnp.concatenate([jnp.where(left, a, swap(b)), jnp.where(left, swap(a), b)], axis=0))
+    return jnp.concatenate(tiles, axis=1)
+
+
 def qkv_kernel(x_ref, small_ref, wq_ref, wk_ref, wv_ref, o_ref, s_ref):
-    tp = x_ref.shape[0] // 16
-    left = left_half((16, 128))
-    tiles = []
-    total = jnp.zeros((32, 128), f32)
-    for i in range(tp // 2):
-        a = x_ref[32 * i : 32 * i + 16, :].astype(f32)
-        b = x_ref[32 * i + 16 : 32 * i + 32, :].astype(f32)
-        tile = jnp.concatenate(
-            [jnp.where(left, a, swap(b)), jnp.where(left, swap(a), b)], axis=0
-        )
-        total = total + tile * tile
-        tiles.append(tile)
-    width = 64.0 * tp
-    scale = lax.rsqrt(jnp.sum(total, axis=1, keepdims=True) / width + EPS)
-    normed = jnp.concatenate(
-        [(tile * scale * small_ref[MIX + i : MIX + i + 1, :]).astype(bf16) for i, tile in enumerate(tiles)],
-        axis=1,
-    )
+    rows = 16
+    tp = x_ref.shape[0] // rows
+    hidden = normed_rows(x_ref, small_ref, MIX, rows, tp)
     w = jnp.concatenate([wq_ref[...], wk_ref[...], wv_ref[...]], axis=0)
-    out = nt(normed, w)
+    out = nt(hidden, w)
     v = out[:, 128:192]
     s_ref[pl.ds(0, 32, stride=2), :] = out[:, :128]
     s_ref[pl.ds(1, 32, stride=2), :] = jnp.concatenate([v, jnp.zeros_like(v)], axis=1)
@@ -167,10 +175,8 @@
     wide = jnp.concatenate(
         [jnp.where(first_map, qu, 0.0), jnp.where(first_map, 0.0, qu)], axis=1
     )
-    scores = jnp.zeros((rows, length), f32)
-    for h in range(heads):
-        lhs = jnp.where(row // 2 == h, wide, 0.0).astype(bf16)
-        scores = scores + nt(lhs, ck_ref[h])
+    wideb = wide.astype(bf16)
+    scores = jnp.concatenate([nt(wideb[2 * h : 2 * h + 2], ck_ref[h]) for h in range(heads)], axis=0)
     scale = 128.0 ** -0.5
     scores = scores * scale
     own = jnp.sum(qu * ku, axis=1, keepdims=True) * scale
@@ -192,10 +198,10 @@
     ]
     past_mix = jnp.concatenate(mixes[:2], axis=1)[:, 0:length]
     own_mix = mixes[2][:, 0:1].astype(bf16).astype(f32)
-    out = own_mix * new_value.astype(bf16).astype(f32)
-    for h in range(heads):
-        lhs = jnp.where(head == h, past_mix, 0.0).astype(bf16)
-        out = out + nn(lhs, cv_ref[h])
+    mixb = past_mix.astype(bf16)
+    out = own_mix * new_value.astype(bf16).astype(f32) + jnp.concatenate(
+        [nn(mixb[h : h + 1], cv_ref[h]) for h in range(heads)], axis=0
+    )
     r = lax.rsqrt(jnp.mean(out * out, axis=1, keepdims=True) + EPS)
     sub = jnp.concatenate([small_ref[SG : SG + 1, :], small_ref[SG + 1 : SG + 2, :]], axis=1)
     mixed = (out * r * sub * OUT_FACTOR).astype(bf16)
@@ -230,25 +236,7 @@
     rows = 64
     tp = x_ref.shape[0] // rows
     left = left_half((rows, 128))
-    left_row = left_half((1, 128))
-    total = jnp.zeros((rows, 128), f32)
-    for i in range(tp):
-        x = x_ref[rows * i : rows * (i + 1), :].astype(f32)
-        total = total + x * x
-    sums = [jnp.sum(jnp.where(left == keep, total, 0.0), axis=1, keepdims=True) for keep in (True, False)]
-    scales = [lax.rsqrt(v / (64.0 * tp) + EPS) for v in sums]
-    scale = jnp.where(left, scales[0], scales[1])
-    tiles = []
-    for i in range(tp // 2):
-        gain = small_ref[FFN + i : FFN + i + 1, :]
-        turned = swap(gain)
-        gains = (jnp.where(left_row, gain, turned), jnp.where(left_row, turned, gain))
-        a, b = [
-            (x_ref[rows * (2 * i + j) : rows * (2 * i + j + 1), :].astype(f32) * scale * gains[j]).astype(bf16)
-            for j in (0, 1)
-        ]
-        tiles.append(jnp.concatenate([jnp.where(left, a, swap(b)), jnp.where(left, swap(a), b)], axis=0))
-    hidden = jnp.concatenate(tiles, axis=1)
+    hidden = normed_rows(x_ref, small_ref, FFN, rows, tp)
     both = nn(hidden, jnp.concatenate([wg_ref[...], wu_ref[...]], axis=1))
     gate = both[:, :128]
     act = (gate / (1.0 + jnp.exp(-gate)) * both[:, 128:]).astype(bf16)

time: 144 us -> 144 us (level)
  no operation moved by 1% of the time
where the time goes in v5:
time: 144 us; the launch traced here: 143 us
  blocking collectives  137 us (95%)
  Pallas kernels  4.09 us (3%)
  between operations  1.46 us (1%)
    all_to_all x7, blocking collectives, exchange(): lax.all_to_all(x.reshape(n, rows // n, lanes), axis, split_axis=0, concat...  137 us

profile of v5, /device:TPU:1, one launch (start us, length us, event | category | flops | bytes accessed | tf_op | source)
XLA Modules:
  0.0 143.4 jit_solution(1757797554747986791)
XLA Ops:
  1.4 0.0 copy-start.12
  1.4 0.0 copy-start.15
  1.4 0.6 copy-done.10
  2.0 0.0 copy-done.11
  2.0 0.0 copy-done.14
  2.0 0.0 copy-done.17
  2.0 0.1 copy-done.9
  2.1 0.1 pack.1
  2.2 19.8 %all_to_all.35 = bf16[32,16,128]{2,1,0:T(8,128)(2,1)S(1)} all-to-all(bf16[32,16,128]{2,1,0:T(8,128)(2,1)S(1)} %bitcast.37), channel_id=1, replica_groups=mesh['ep'=32,'tp'=32] {'tp'}, dimensions={0} | all-to-all | bytes 262144 | tf_op jit(solution)/shard_map/all_to_all | solution.py:297
  22.0 0.0 copy-start
  22.0 0.5 qkv.1
  22.5 11.6 %all_to_all.36 = bf16[32,2,128]{2,1,0:T(2,128)(2,1)S(1)} all-to-all(bf16[32,2,128]{2,1,0:T(2,128)(2,1)S(1)} %bitcast.42), channel_id=1, replica_groups=mesh['ep'=32,'tp'=32] {'tp'}, dimensions={0} | all-to-all | bytes 32768 | tf_op jit(solution)/shard_map/all_to_all | solution.py:297
  34.2 1.0 attend.1
  35.2 12.5 %all_to_all.37 = bf16[32,8,256]{2,1,0:T(8,128)(2,1)S(1)} all-to-all(bf16[32,8,256]{2,1,0:T(8,128)(2,1)S(1)} %bitcast.35), channel_id=1, replica_groups=mesh['ep'=32,'tp'=32] {'tp'}, dimensions={0} | all-to-all | bytes 262144 | tf_op jit(solution)/shard_map/all_to_all | solution.py:297
  47.7 0.4 project.1
  48.1 0.0 copy-start.4
  48.1 35.3 %all_to_all.38 = bf16[32,2,128]{2,1,0:T(2,128)(2,1)S(1)} all-to-all(bf16[32,2,128]{2,1,0:T(2,128)(2,1)S(1)} %bitcast.41), channel_id=1, replica_groups=mesh['ep'=32,'tp'=32] {'ep'}, dimensions={0} | all-to-all | bytes 32768 | tf_op jit(solution)/shard_map/all_to_all | solution.py:297
  83.5 0.1 broadcast_in_dim.9
  83.6 18.8 %all_to_all.39 = bf16[32,64,128]{2,1,0:T(8,128)(2,1)S(1)} all-to-all(bf16[32,64,128]{2,1,0:T(8,128)(2,1)S(1)} %broadcast_in_dim.9), channel_id=1, replica_groups=mesh['ep'=32,'tp'=32] {'tp'}, dimensions={0} | all-to-all | bytes 1048576 | tf_op jit(solution)/shard_map/all_to_all | solution.py:297
  102.4 1.2 expert.1
  103.6 20.8 %all_to_all.40 = bf16[32,64,128]{2,1,0:T(8,128)(2,1)S(1)} all-to-all(bf16[32,64,128]{2,1,0:T(8,128)(2,1)S(1)} %bitcast.33), channel_id=1, replica_groups=mesh['ep'=32,'tp'=32] {'tp'}, dimensions={0} | all-to-all | bytes 1048576 | tf_op jit(solution)/shard_map/all_to_all | solution.py:297
  124.4 0.1 sum.1
  124.5 18.1 %all_to_all.41 = bf16[32,2,128]{2,1,0:T(2,128)(2,1)S(1)} all-to-all(bf16[32,2,128]{2,1,0:T(2,128)(2,1)S(1)} %bitcast.43), channel_id=1, replica_groups=mesh['ep'=32,'tp'=32] {'ep'}, dimensions={0} | all-to-all | bytes 32768 | tf_op jit(solution)/shard_map/all_to_all | solution.py:297
  142.6 0.8 combine.1
  (28 shorter events, 0.1 us)
Async XLA Ops:
  1.3 0.7 copy-start.10
  1.3 0.7 copy-start.11
  1.3 0.7 copy-start.13
  1.3 0.7 copy-start.14
  1.3 0.7 copy-start.16
  1.3 0.7 copy-start.17
  1.3 0.7 copy-start.9
  1.4 0.7 copy-start.12
  1.4 0.7 copy-start.15
  2.1 19.9 %copy-start.6 = (bf16[2048,64]{0,1:T(8,128)(2,1)S(1)}, bf16[2048,64]{0,1:T(8,128)(2,1)}, u32[]{:S(2)}) copy-start(bf16[2048,64]{0,1:T(8,128)(2,1)} %param.30) | copy-start | bytes 786436
  2.1 19.9 %copy-start.7 = (bf16[2048,64]{0,1:T(8,128)(2,1)S(1)}, bf16[2048,64]{0,1:T(8,128)(2,1)}, u32[]{:S(2)}) copy-start(bf16[2048,64]{0,1:T(8,128)(2,1)} %param.31) | copy-start | bytes 786436
  2.2 19.8 %copy-start.5 = (bf16[2048,64]{0,1:T(8,128)(2,1)S(1)}, bf16[2048,64]{0,1:T(8,128)(2,1)}, u32[]{:S(2)}) copy-start(bf16[2048,64]{0,1:T(8,128)(2,1)} %param.29) | copy-start | bytes 786436
  22.0 12.2 %copy-start = (bf16[1,8,224,256]{3,2,1,0:T(8,128)(2,1)S(1)}, bf16[1,8,224,256]{3,2,1,0:T(8,128)(2,1)}, u32[]{:S(2)}) copy-start(bf16[1,8,224,256]{3,2,1,0:T(8,128)(2,1)} %param.20) | copy-start | bytes 2752516
  22.0 12.2 %copy-start.1 = (bf16[1,8,224,256]{3,2,1,0:T(8,128)(2,1)S(1)}, bf16[1,8,224,256]{3,2,1,0:T(8,128)(2,1)}, u32[]{:S(2)}) copy-start(bf16[1,8,224,256]{3,2,1,0:T(8,128)(2,1)} %param.21) | copy-start | bytes 2752516
  35.2 12.5 %copy-start.8 = (bf16[2048,64]{0,1:T(8,128)(2,1)S(1)}, bf16[2048,64]{0,1:T(8,128)(2,1)}, u32[]{:S(2)}) copy-start(bf16[2048,64]{0,1:T(8,128)(2,1)} %param.32) | copy-start | bytes 786436
  48.1 54.3 %copy-start.4 = (bf16[1,128,2048]{2,1,0:T(8,128)(2,1)S(1)}, bf16[1,128,2048]{2,1,0:T(8,128)(2,1)}, u32[]{:S(2)}) copy-start(bf16[1,128,2048]{2,1,0:T(8,128)(2,1)} %param.37) | copy-start | bytes 1572868
  83.6 18.8 %copy-start.2 = (bf16[1,2048,128]{2,1,0:T(8,128)(2,1)S(1)}, bf16[1,2048,128]{2,1,0:T(8,128)(2,1)}, u32[]{:S(2)}) copy-start(bf16[1,2048,128]{2,1,0:T(8,128)(2,1)} %param.35) | copy-start | bytes 1572868
  83.6 18.8 %copy-start.3 = (bf16[1,2048,128]{2,1,0:T(8,128)(2,1)S(1)}, bf16[1,2048,128]{2,1,0:T(8,128)(2,1)}, u32[]{:S(2)}) copy-start(bf16[1,2048,128]{2,1,0:T(8,128)(2,1)} %param.36) | copy-start | bytes 1572868

commit v6 on v5

--- a/solution.py
+++ b/solution.py
@@ -237,9 +237,9 @@
     tp = x_ref.shape[0] // rows
     left = left_half((rows, 128))
     hidden = normed_rows(x_ref, small_ref, FFN, rows, tp)
-    both = nn(hidden, jnp.concatenate([wg_ref[...], wu_ref[...]], axis=1))
-    gate = both[:, :128]
-    act = (gate / (1.0 + jnp.exp(-gate)) * both[:, 128:]).astype(bf16)
+    gate = nn(hidden, wg_ref[...])
+    up = nn(hidden, wu_ref[...])
+    act = (gate / (1.0 + jnp.exp(-gate)) * up).astype(bf16)
     for i in range(tp // 2):
         if i % 2 == 0:
             pair = nn(act, wd_ref[:, 128 * i : 128 * (i + 2)])

time: 144 us -> 144 us (level)
  no operation moved by 1% of the time
where the time goes in v6:
time: 144 us; the launch traced here: 143 us
  blocking collectives  137 us (95%)
  Pallas kernels  3.99 us (3%)
  between operations  1.46 us (1%)
    all_to_all x7, blocking collectives, exchange(): lax.all_to_all(x.reshape(n, rows // n, lanes), axis, split_axis=0, concat...  137 us

profile of v6, /device:TPU:1, one launch (start us, length us, event | category | flops | bytes accessed | tf_op | source)
XLA Modules:
  0.0 143.3 jit_solution(8367163278597936264)
XLA Ops:
  1.4 0.0 copy-start.12
  1.4 0.0 copy-start.15
  1.4 0.6 copy-done.10
  2.0 0.0 copy-done.11
  2.0 0.0 copy-done.14
  2.0 0.0 copy-done.17
  2.0 0.1 copy-done.9
  2.1 0.1 pack.1
  2.2 19.8 %all_to_all.35 = bf16[32,16,128]{2,1,0:T(8,128)(2,1)S(1)} all-to-all(bf16[32,16,128]{2,1,0:T(8,128)(2,1)S(1)} %bitcast.37), channel_id=1, replica_groups=mesh['ep'=32,'tp'=32] {'tp'}, dimensions={0} | all-to-all | bytes 262144 | tf_op jit(solution)/shard_map/all_to_all | solution.py:297
  22.0 0.0 copy-start
  22.0 0.5 qkv.1
  22.5 11.6 %all_to_all.36 = bf16[32,2,128]{2,1,0:T(2,128)(2,1)S(1)} all-to-all(bf16[32,2,128]{2,1,0:T(2,128)(2,1)S(1)} %bitcast.42), channel_id=1, replica_groups=mesh['ep'=32,'tp'=32] {'tp'}, dimensions={0} | all-to-all | bytes 32768 | tf_op jit(solution)/shard_map/all_to_all | solution.py:297
  34.2 1.0 attend.1
  35.2 12.5 %all_to_all.37 = bf16[32,8,256]{2,1,0:T(8,128)(2,1)S(1)} all-to-all(bf16[32,8,256]{2,1,0:T(8,128)(2,1)S(1)} %bitcast.35), channel_id=1, replica_groups=mesh['ep'=32,'tp'=32] {'tp'}, dimensions={0} | all-to-all | bytes 262144 | tf_op jit(solution)/shard_map/all_to_all | solution.py:297
  47.7 0.4 project.1
  48.1 0.0 copy-start.4
  48.1 35.3 %all_to_all.38 = bf16[32,2,128]{2,1,0:T(2,128)(2,1)S(1)} all-to-all(bf16[32,2,128]{2,1,0:T(2,128)(2,1)S(1)} %bitcast.41), channel_id=1, replica_groups=mesh['ep'=32,'tp'=32] {'ep'}, dimensions={0} | all-to-all | bytes 32768 | tf_op jit(solution)/shard_map/all_to_all | solution.py:297
  83.5 0.1 broadcast_in_dim.9
  83.6 18.8 %all_to_all.39 = bf16[32,64,128]{2,1,0:T(8,128)(2,1)S(1)} all-to-all(bf16[32,64,128]{2,1,0:T(8,128)(2,1)S(1)} %broadcast_in_dim.9), channel_id=1, replica_groups=mesh['ep'=32,'tp'=32] {'tp'}, dimensions={0} | all-to-all | bytes 1048576 | tf_op jit(solution)/shard_map/all_to_all | solution.py:297
  102.4 1.1 expert.1
  103.5 20.8 %all_to_all.40 = bf16[32,64,128]{2,1,0:T(8,128)(2,1)S(1)} all-to-all(bf16[32,64,128]{2,1,0:T(8,128)(2,1)S(1)} %bitcast.33), channel_id=1, replica_groups=mesh['ep'=32,'tp'=32] {'tp'}, dimensions={0} | all-to-all | bytes 1048576 | tf_op jit(solution)/shard_map/all_to_all | solution.py:297
  124.3 0.1 sum.1
  124.4 18.1 %all_to_all.41 = bf16[32,2,128]{2,1,0:T(2,128)(2,1)S(1)} all-to-all(bf16[32,2,128]{2,1,0:T(2,128)(2,1)S(1)} %bitcast.43), channel_id=1, replica_groups=mesh['ep'=32,'tp'=32] {'ep'}, dimensions={0} | all-to-all | bytes 32768 | tf_op jit(solution)/shard_map/all_to_all | solution.py:297
  142.5 0.8 combine.1
  (28 shorter events, 0.1 us)
Async XLA Ops:
  1.3 0.7 copy-start.10
  1.3 0.7 copy-start.11
  1.3 0.7 copy-start.13
  1.3 0.7 copy-start.14
  1.3 0.7 copy-start.16
  1.3 0.7 copy-start.17
  1.3 0.7 copy-start.9
  1.4 0.7 copy-start.12
  1.4 0.7 copy-start.15
  2.1 19.9 %copy-start.6 = (bf16[2048,64]{0,1:T(8,128)(2,1)S(1)}, bf16[2048,64]{0,1:T(8,128)(2,1)}, u32[]{:S(2)}) copy-start(bf16[2048,64]{0,1:T(8,128)(2,1)} %param.30) | copy-start | bytes 786436
  2.1 19.9 %copy-start.7 = (bf16[2048,64]{0,1:T(8,128)(2,1)S(1)}, bf16[2048,64]{0,1:T(8,128)(2,1)}, u32[]{:S(2)}) copy-start(bf16[2048,64]{0,1:T(8,128)(2,1)} %param.31) | copy-start | bytes 786436
  2.2 19.8 %copy-start.5 = (bf16[2048,64]{0,1:T(8,128)(2,1)S(1)}, bf16[2048,64]{0,1:T(8,128)(2,1)}, u32[]{:S(2)}) copy-start(bf16[2048,64]{0,1:T(8,128)(2,1)} %param.29) | copy-start | bytes 786436
  22.0 12.2 %copy-start = (bf16[1,8,224,256]{3,2,1,0:T(8,128)(2,1)S(1)}, bf16[1,8,224,256]{3,2,1,0:T(8,128)(2,1)}, u32[]{:S(2)}) copy-start(bf16[1,8,224,256]{3,2,1,0:T(8,128)(2,1)} %param.20) | copy-start | bytes 2752516
  22.0 12.2 %copy-start.1 = (bf16[1,8,224,256]{3,2,1,0:T(8,128)(2,1)S(1)}, bf16[1,8,224,256]{3,2,1,0:T(8,128)(2,1)}, u32[]{:S(2)}) copy-start(bf16[1,8,224,256]{3,2,1,0:T(8,128)(2,1)} %param.21) | copy-start | bytes 2752516
  35.2 12.5 %copy-start.8 = (bf16[2048,64]{0,1:T(8,128)(2,1)S(1)}, bf16[2048,64]{0,1:T(8,128)(2,1)}, u32[]{:S(2)}) copy-start(bf16[2048,64]{0,1:T(8,128)(2,1)} %param.32) | copy-start | bytes 786436
  48.1 54.3 %copy-start.4 = (bf16[1,128,2048]{2,1,0:T(8,128)(2,1)S(1)}, bf16[1,128,2048]{2,1,0:T(8,128)(2,1)}, u32[]{:S(2)}) copy-start(bf16[1,128,2048]{2,1,0:T(8,128)(2,1)} %param.37) | copy-start | bytes 1572868
  83.6 18.8 %copy-start.2 = (bf16[1,2048,128]{2,1,0:T(8,128)(2,1)S(1)}, bf16[1,2048,128]{2,1,0:T(8,128)(2,1)}, u32[]{:S(2)}) copy-start(bf16[1,2048,128]{2,1,0:T(8,128)(2,1)} %param.35) | copy-start | bytes 1572868
  83.6 18.8 %copy-start.3 = (bf16[1,2048,128]{2,1,0:T(8,128)(2,1)S(1)}, bf16[1,2048,128]{2,1,0:T(8,128)(2,1)}, u32[]{:S(2)}) copy-start(bf16[1,2048,128]{2,1,0:T(8,128)(2,1)} %param.36) | copy-start | bytes 1572868
